TPU v7x, 32 devices: a whole 2x2x4 slice. The times are simulated.
32 devices in a mesh: sp: 4 (over z), fs: 4 (over y, x), tp: 2 (over core).
Axes of the slice: x: 2, y: 2, z: 4, core: 2. Of those that a mesh axis runs over, the one named last changes fastest.
Arguments:
- tokens: bfloat16 [4, 512, 2048], P('fs', 'sp'), may hold values from -6 to 6
- norm_gain: float32 [2048], replicated, may hold values from 0.1 to 1.9
- w_ret_query: bfloat16 [2048, 2048], P(('sp', 'fs'), 'tp'), may hold values from -0.125 to 0.125
- w_ret_key: bfloat16 [2048, 2048], P(('sp', 'fs'), 'tp'), may hold values from -0.125 to 0.125
- w_ret_value: bfloat16 [2048, 2048], P(('sp', 'fs'), 'tp'), may hold values from -0.125 to 0.125
- w_q_down: bfloat16 [2048, 768], P(('sp', 'fs'), 'tp'), may hold values from -0.125 to 0.125
- w_kv_down: bfloat16 [2048, 512], P(('sp', 'fs'), 'tp'), may hold values from -0.125 to 0.125
- w_rope_key: bfloat16 [2048, 64], P(('sp', 'fs')), may hold values from -0.125 to 0.125
- w_q_up: bfloat16 [768, 3072], P(None, 'tp'), may hold values from -0.21875 to 0.21875
- w_kv_up: bfloat16 [512, 4096], P(None, 'tp'), may hold values from -0.25 to 0.25
- q_lat_gain: float32 [768], replicated, may hold values from 0.4 to 10
- kv_lat_gain: float32 [512], replicated, may hold values from 0.4 to 10
- att_norm_gain: float32 [2048], P('tp'), may hold values from 0.1 to 1.9
- ret_norm_gain: float32 [2048], P('tp'), may hold values from 0.1 to 1.9
- w_ret_out: bfloat16 [2048, 2048], P(('sp', 'fs'), 'tp'), may hold values from -0.09375 to 0.09375
- w_att_out: bfloat16 [2048, 2048], P(('sp', 'fs'), 'tp'), may hold values from -0.09375 to 0.09375
- head_rate: float32 [8], P('tp'), may hold values from -0.05 to 0
- decay_shift: float32 [4, 8, 512], P('fs', 'tp', 'sp'), may hold values from -1.1 to 0
- start_state: float32 [4, 8, 256, 256], P('fs', 'tp'), may hold values from -20 to 20
Outputs:
- mixed: bfloat16 [4, 512, 2048], P('fs', ('sp', 'tp'))
All inputs are finite; a program needn't handle non-finite values.
Results may differ from a plain program's by a relative error of at most 0.018.
The roundings to bfloat16 on the way count: a program that leaves them out, or rounds other values in their place, can miss the bound.
Values may be sent and summed in bfloat16 or wider, within the bound.
A program may use at most 64 MiB of HBM per device.

v0:
```python
import jax
import jax.numpy as jnp
from jax import lax
from jax.sharding import PartitionSpec as P

RET_DIM = 256
NOPE_DIM = 128
ROPE_DIM = 64
VAL_DIM = 128
KV_LAT = 512


EPSILON = 1e-06
THETA_BASE = 10000.0
TOP_PRECISION = lax.Precision.HIGHEST


def prefix(x, axis, combine, identity):
    peers, position = (lax.axis_size(axis), lax.axis_index(axis))
    everything = jax.tree.map(
        lambda part, kind: lax.all_gather(part.astype(kind), axis), x, (jnp.bfloat16, jnp.bfloat16)
    )
    start = jax.tree.map(
        lambda part, zero: jnp.broadcast_to(jnp.asarray(zero, part.dtype), part.shape), x, identity
    )

    def lap(k, before):
        reached = k < position
        new = combine(
            before, jax.tree.map(lambda part, own: part[k].astype(own.dtype), everything, x)
        )
        return jax.tree.map(lambda a, b: jnp.where(reached, a, b), new, before)

    return lax.fori_loop(0, peers, lap, start)


def angle_tables(positions, rot_width):
    half_width = rot_width // 2
    inverse = THETA_BASE ** (-jnp.arange(half_width, dtype=jnp.float32) * 2.0 / rot_width)
    angles = positions.astype(jnp.float32)[:, None] * inverse[None, :]
    return (jnp.cos(angles), jnp.sin(angles))


def rotate(values, cosine, sine):
    half_width = values.shape[-1] // 2
    front_half = values[..., :half_width]
    back_half = values[..., half_width:]
    return jnp.concatenate(
        [front_half * cosine - back_half * sine, back_half * cosine + front_half * sine], axis=-1
    )


def rms_scale(values, gain_vector):
    return (
        values
        * lax.rsqrt(jnp.mean(values * values, axis=-1, keepdims=True) + EPSILON)
        * gain_vector
    )


def chain_states(earlier, later):
    early_log, early_state = earlier
    late_log, late_state = later
    return (early_log + late_log, jnp.exp(late_log)[:, None, None] * early_state + late_state)


def per_device(
    tokens,
    norm_gain,
    w_ret_query,
    w_ret_key,
    w_ret_value,
    w_q_down,
    w_kv_down,
    w_rope_key,
    w_q_up,
    w_kv_up,
    q_lat_gain,
    kv_lat_gain,
    att_norm_gain,
    ret_norm_gain,
    w_ret_out,
    w_att_out,
    head_rate,
    decay_shift,
    start_state,
):
    tok_rows = tokens.shape[1]
    ret_local = head_rate.shape[0]
    att_local = w_q_up.shape[1] // (NOPE_DIM + ROPE_DIM)
    row_offset = lax.axis_index("sp") * tok_rows
    positions = row_offset + jnp.arange(tok_rows, dtype=jnp.int32)
    (
        full_query,
        full_key,
        full_value,
        full_q_down,
        full_kv_down,
        full_rope,
        full_ret_out,
        full_att_out,
    ) = (
        lax.all_gather(w_ret_query, ("sp", "fs"), axis=0, tiled=True),
        lax.all_gather(w_ret_key, ("sp", "fs"), axis=0, tiled=True),
        lax.all_gather(w_ret_value, ("sp", "fs"), axis=0, tiled=True),
        lax.all_gather(w_q_down, ("sp", "fs"), axis=0, tiled=True),
        lax.all_gather(w_kv_down, ("sp", "fs"), axis=0, tiled=True),
        lax.all_gather(w_rope_key, ("sp", "fs"), axis=0, tiled=True),
        lax.all_gather(w_ret_out, ("sp", "fs"), axis=0, tiled=True),
        lax.all_gather(w_att_out, ("sp", "fs"), axis=0, tiled=True),
    )
    source = tokens[0].astype(jnp.float32)
    normed = rms_scale(source, norm_gain).astype(jnp.bfloat16)
    ret_cos, ret_sin = angle_tables(positions, RET_DIM)
    rope_cos, rope_sin = angle_tables(positions, ROPE_DIM)

    def project(weight):
        return jnp.dot(normed, weight, preferred_element_type=jnp.float32)

    part_q = project(full_q_down).astype(jnp.bfloat16)
    part_kv = project(full_kv_down).astype(jnp.bfloat16)
    lat_q_raw, lat_kv_raw = (
        lax.all_gather(part_q, "tp", axis=1, tiled=True),
        lax.all_gather(part_kv, "tp", axis=1, tiled=True),
    )
    retention_query = rotate(
        project(full_query).reshape(tok_rows, ret_local, RET_DIM),
        ret_cos[:, None],
        ret_sin[:, None],
    ).astype(jnp.bfloat16)
    retention_key = (
        rotate(
            project(full_key).reshape(tok_rows, ret_local, RET_DIM),
            ret_cos[:, None],
            ret_sin[:, None],
        )
        * RET_DIM ** (-0.5)
    ).astype(jnp.bfloat16)
    retention_value = project(full_value).reshape(tok_rows, ret_local, RET_DIM).astype(jnp.bfloat16)
    rope_key = rotate(project(full_rope), rope_cos, rope_sin).astype(jnp.bfloat16)
    log_rates = head_rate[:, None] + decay_shift[0]
    cumul = jnp.cumsum(log_rates, axis=1)
    offsets = jnp.arange(tok_rows, dtype=jnp.int32)
    lower_mask = offsets[None, :] <= offsets[:, None]
    decay_matrix = jnp.exp(
        jnp.where(lower_mask[None], cumul[:, :, None] - cumul[:, None, :], -jnp.inf)
    )
    block_score_grid = (
        jnp.einsum(
            "zgq,ugq->gzu", retention_query, retention_key, preferred_element_type=jnp.float32
        )
        * decay_matrix
    ).astype(jnp.bfloat16)
    inside_block_output = jnp.einsum(
        "vzs,svp->zvp", block_score_grid, retention_value, preferred_element_type=jnp.float32
    )
    block_output_sum = cumul[:, -1]
    weighted_values = (
        retention_key.astype(jnp.float32) * jnp.exp(block_output_sum[:, None] - cumul).T[:, :, None]
    )
    contribution = jnp.einsum(
        "uzj,uzv->zjv",
        weighted_values,
        retention_value.astype(jnp.float32),
        precision=TOP_PRECISION,
    )
    identity = (jnp.zeros_like(block_output_sum), jnp.zeros_like(contribution))
    before_log, before_state = prefix(
        (block_output_sum, contribution), "sp", chain_states, identity
    )
    q_latent = rms_scale(lat_q_raw.astype(jnp.float32), q_lat_gain).astype(jnp.bfloat16)
    kv_latent = rms_scale(lat_kv_raw.astype(jnp.float32), kv_lat_gain).astype(jnp.bfloat16)
    query_full = jnp.dot(q_latent, w_q_up, preferred_element_type=jnp.float32).reshape(
        tok_rows, att_local, NOPE_DIM + ROPE_DIM
    )
    query_nope = query_full[..., :NOPE_DIM].astype(jnp.bfloat16)
    query_rope = rotate(query_full[..., NOPE_DIM:], rope_cos[:, None], rope_sin[:, None]).astype(
        jnp.bfloat16
    )
    att_scale = (NOPE_DIM + ROPE_DIM) ** (-0.5)

    def attend(carry, key_nope, key_values, key_rope, start):
        running_max, running_sum, running_acc = carry
        key_count = key_rope.shape[0]
        score_matrix = (
            jnp.einsum("qhd,khd->hqk", query_nope, key_nope, preferred_element_type=jnp.float32)
            + jnp.einsum("qhd,kd->hqk", query_rope, key_rope, preferred_element_type=jnp.float32)
        ) * att_scale
        key_positions = start + jnp.arange(key_count, dtype=jnp.int32)
        allowed = key_positions[None, :] <= positions[:, None]
        masked = jnp.where(allowed[None], score_matrix, -jnp.inf)
        new_max = jnp.maximum(running_max, jnp.max(masked, axis=-1))
        safe_max = jnp.where(jnp.isfinite(new_max), new_max, 0.0)
        weights = jnp.exp(masked - safe_max[..., None])
        rescale = jnp.exp(running_max - safe_max)
        new_sum = running_sum * rescale + jnp.sum(weights, axis=-1)
        new_acc = running_acc * rescale[..., None] + jnp.einsum(
            "hqk,khd->hqd",
            weights.astype(jnp.bfloat16),
            key_values,
            preferred_element_type=jnp.float32,
        )
        return (new_max, new_sum, new_acc)

    def expand_attend(carry_in, lat_piece, rope_piece, start):
        wide = (
            jnp.dot(lat_piece, w_kv_up, preferred_element_type=jnp.float32)
            .astype(jnp.bfloat16)
            .reshape(rope_piece.shape[0], att_local, NOPE_DIM + VAL_DIM)
        )
        return attend(carry_in, wide[..., :NOPE_DIM], wide[..., NOPE_DIM:], rope_piece, start)

    empty = (
        jnp.full((att_local, tok_rows), -jnp.inf, jnp.float32),
        jnp.zeros((att_local, tok_rows), jnp.float32),
        jnp.zeros((att_local, tok_rows, VAL_DIM), jnp.float32),
    )
    groups = lax.axis_size("tp")
    kv_part = KV_LAT // groups
    rope_part = ROPE_DIM // groups
    my_group = lax.axis_index("tp")
    joined = jnp.concatenate(
        [
            lax.dynamic_slice_in_dim(kv_latent, my_group * kv_part, kv_part, 1),
            lax.dynamic_slice_in_dim(rope_key, my_group * rope_part, rope_part, 1),
        ],
        axis=1,
    )
    all_rows = lax.all_gather(joined, "sp", axis=0, tiled=True)
    complete = lax.all_gather(all_rows, "tp", axis=1, tiled=True)
    total_rows = complete.shape[0]
    grouped = complete.reshape(total_rows, groups, kv_part + rope_part)
    lat_all = grouped[:, :, :kv_part].reshape(total_rows, KV_LAT)
    rope_all = grouped[:, :, kv_part:].reshape(total_rows, ROPE_DIM)

    def visit(block_index, carry_in):
        start = block_index * tok_rows
        lat_piece = lax.dynamic_slice_in_dim(lat_all, start, tok_rows, 0)
        rope_piece = lax.dynamic_slice_in_dim(rope_all, start, tok_rows, 0)
        return expand_attend(carry_in, lat_piece, rope_piece, start)

    final = lax.fori_loop(0, lax.axis_index("sp") + 1, visit, empty)
    att_raw = jnp.transpose(final[2] / final[1][..., None], (1, 0, 2))
    att_out = (
        rms_scale(att_raw, att_norm_gain.reshape(att_local, VAL_DIM))
        .astype(jnp.bfloat16)
        .reshape(tok_rows, att_local * VAL_DIM)
    )
    entering = jnp.exp(before_log)[:, None, None] * start_state[0] + before_state
    carried_term = (
        jnp.einsum(
            "nhd,hde->nhe", retention_query.astype(jnp.float32), entering, precision=TOP_PRECISION
        )
        * jnp.exp(cumul).T[:, :, None]
    )
    ret_raw = inside_block_output + carried_term
    row_mean = jnp.mean(ret_raw, axis=-1, keepdims=True)
    centered = ret_raw - row_mean
    row_var = jnp.mean(centered * centered, axis=-1, keepdims=True)
    ret_out = (
        (centered * lax.rsqrt(row_var + EPSILON) * ret_norm_gain.reshape(ret_local, RET_DIM))
        .astype(jnp.bfloat16)
        .reshape(tok_rows, ret_local * RET_DIM)
    )
    contract = (((1,), (1,)), ((), ()))
    mixed = lax.psum_scatter(
        (
            lax.dot_general(ret_out, full_ret_out, contract, preferred_element_type=jnp.float32)
            + lax.dot_general(att_out, full_att_out, contract, preferred_element_type=jnp.float32)
        ).astype(jnp.bfloat16),
        "tp",
        scatter_dimension=0,
        tiled=True,
    )
    return mixed[None]


def solution(mesh):
    placed = (
        P("fs", "sp", None),
        P(),
        P(("sp", "fs"), "tp"),
        P(("sp", "fs"), "tp"),
        P(("sp", "fs"), "tp"),
        P(("sp", "fs"), "tp"),
        P(("sp", "fs"), "tp"),
        P(("sp", "fs"), None),
        P(None, "tp"),
        P(None, "tp"),
        P(),
        P(),
        P("tp"),
        P("tp"),
        P(("sp", "fs"), "tp"),
        P(("sp", "fs"), "tp"),
        P("tp"),
        P("fs", "tp", "sp"),
        P("fs", "tp", None, None),
    )
    return jax.shard_map(
        per_device,
        mesh=mesh,
        in_specs=placed,
        out_specs=P("fs", ("sp", "tp"), None),
        check_vma=False,
    )
```

profile of v0, /device:TPU:0, one launch (start us, length us, event | category | flops | bytes accessed | tf_op | source)
XLA Modules:
  0.0 576.8 jit_solution(4577813342815641826)
XLA Ops:
  13.4 75.1 %all-gather.11.cloned.1.call-done = bf16[2048,1024]{1,0:T(8,128)(2,1)} async-done(((bf16[128,1024]{1,0:T(8,128)(2,1)}), bf16[2048,1024]{1,0:T(8,128)(2,1)}) %all-gather.11.cloned.1.call-update) | async-done | bytes 4194320 | tf_op jit(solution)/shard_map/all_gather | solution.py:105
  88.5 6.5 %copy.76 = bf16[1024,2048]{1,0:T(8,128)(2,1)} copy(bf16[1024,2048]{0,1:T(8,128)(2,1)} %bitcast.130) | data formatting | bytes 8388608 | tf_op jit(solution)/shard_map/dot_general | solution.py:118
  94.9 70.5 %all-gather.15.cloned.1.call-done = bf16[2048,1024]{1,0:T(8,128)(2,1)} async-done(((bf16[128,1024]{1,0:T(8,128)(2,1)}), bf16[2048,1024]{1,0:T(8,128)(2,1)}) %all-gather.15.cloned.1.call-update) | async-done | bytes 4194320 | tf_op jit(solution)/shard_map/all_gather | solution.py:104
  165.4 6.6 %copy.78 = bf16[1024,2048]{1,0:T(8,128)(2,1)} copy(bf16[1024,2048]{0,1:T(8,128)(2,1)} %bitcast.131) | data formatting | bytes 8388608 | tf_op jit(solution)/shard_map/dot_general | solution.py:118
  172.0 70.4 %all-gather.13.cloned.1.call-done = bf16[2048,1024]{1,0:T(8,128)(2,1)} async-done(((bf16[128,1024]{1,0:T(8,128)(2,1)}), bf16[2048,1024]{1,0:T(8,128)(2,1)}) %all-gather.13.cloned.1.call-update) | async-done | bytes 4194320 | tf_op jit(solution)/shard_map/all_gather | solution.py:103
  242.4 6.5 %copy.77 = bf16[1024,2048]{1,0:T(8,128)(2,1)} copy(bf16[1024,2048]{0,1:T(8,128)(2,1)} %bitcast.132) | data formatting | bytes 8388608 | tf_op jit(solution)/shard_map/dot_general | solution.py:118
  249.0 3.9 fusion.69
  263.0 10.3 %all-reduce = bf16[16]{0:T(256)(128)(2,1)S(1)} all-reduce(bf16[16]{0:T(256)(128)(2,1)S(1)} %dynamic-update-slice), channel_id=2, replica_groups=mesh['sp'=4,'fs'=4,'tp'=2] {'sp'}, use_global_device_ids=true, to_apply=%add | all-reduce | flops 16 | bytes 64
  273.9 39.1 %all_gather.55 = bf16[2048,64]{0,1:T(8,128)(2,1)S(1)} all-gather(bf16[128,64]{0,1:T(8,128)(2,1)S(1)} %copy-done.13), channel_id=1, replica_groups=mesh['sp'=4,'fs'=4,'tp'=2] {'sp','fs'}, dimensions={0}, use_global_device_ids=true | all-gather | bytes 278528 | tf_op jit(solution)/shard_map/all_gather | solution.py:108
  318.7 17.6 %all_gather.56 = bf16[512,288]{1,0:T(8,128)(2,1)} all-gather(bf16[128,288]{1,0:T(8,128)(2,1)S(1)} %pad_maximum_fusion.5), channel_id=1, replica_groups=mesh['sp'=4,'fs'=4,'tp'=2] {'sp'}, dimensions={0}, use_global_device_ids=true | all-gather | bytes 368640 | tf_op jit(solution)/shard_map/all_gather | solution.py:229
  338.1 2.4 all_gather.57
  342.0 17.0 %all-gather.21.cloned.1.call-done = bf16[2048,384]{1,0:T(8,128)(2,1)} async-done(((bf16[128,384]{1,0:T(8,128)(2,1)}), bf16[2048,384]{1,0:T(8,128)(2,1)}) %all-gather.21.cloned.1.call-update) | async-done | bytes 1572880 | tf_op jit(solution)/shard_map/all_gather | solution.py:106
  361.1 2.1 all_gather.59
  369.8 5.2 while.31
  369.8 2.2 convolution_convert_fusion.6
  380.1 2.4 convolution_bitcast_fusion.3
  382.5 22.3 %all-gather.25.cloned.1.call-done = bf16[16,256,256]{2,1,0:T(8,128)(2,1)} async-done(((bf16[4,256,256]{2,1,0:T(8,128)(2,1)}), bf16[16,256,256]{2,1,0:T(8,128)(2,1)}) %all-gather.25.cloned.1.call-update) | async-done | bytes 2097168 | tf_op jit(solution)/shard_map/all_gather | solution.py:21
  404.8 10.5 %while.32 = (s32[]{:T(128)}, f32[4]{0:T(128)}, f32[4,256,256]{2,1,0:T(8,128)S(1)}, s32[]{:T(128)}, bf16[4,4]{1,0:T(4,128)(2,1)}, /*index=5*/bf16[4,4,256,256]{3,2,1,0:T(8,128)(2,1)}, s32[]{:T(128)}, s32[]{:T(128)}) while((s32[]{:T(128)}, f32[4]{0:T(128)}, f32[4,256,256]{2,1,0:T(8,128)S(1)}, s32[]{:T(128)}, bf16[4,4]{1,0:T(4,128)(2,1)}, ...), condition=%wide.region_3.4_spmd.clone, body=%wide.region_2.3_spmd.clone.sunk | while | flops 1310740 | bytes 2621635 | solution.py:34
  416.0 2.6 fusion.80
  419.6 62.4 %all-gather.17.cloned.1.call-done = bf16[2048,1024]{1,0:T(8,128)(2,1)} async-done(((bf16[128,1024]{1,0:T(8,128)(2,1)}), bf16[2048,1024]{1,0:T(8,128)(2,1)}) %all-gather.17.cloned.1.call-update) | async-done | bytes 4194320 | tf_op jit(solution)/shard_map/all_gather | solution.py:109
  482.0 3.8 fusion.81
  485.8 73.2 %all-gather.23.cloned.1.call-done = bf16[2048,1024]{1,0:T(8,128)(2,1)} async-done(((bf16[128,1024]{1,0:T(8,128)(2,1)}), bf16[2048,1024]{1,0:T(8,128)(2,1)}) %all-gather.23.cloned.1.call-update) | async-done | bytes 4194320 | tf_op jit(solution)/shard_map/all_gather | solution.py:110
  559.0 4.6 fusion.17
  563.6 6.7 %reduce-scatter.2.cloned.1.call-done = bf16[64,2048]{1,0:T(8,128)(2,1)} async-done(((bf16[128,2048]{1,0:T(8,128)(2,1)}), bf16[64,2048]{1,0:T(8,128)(2,1)}) %reduce-scatter.2.cloned.1.call-update) | async-done | bytes 262160 | tf_op jit(solution)/shard_map/reduce_scatter | solution.py:266
  (134 shorter events, 54.4 us)
Async XLA Ops:
  6.5 356.8 %copy-start = (bf16[768,1536]{1,0:T(8,128)(2,1)S(1)}, bf16[768,1536]{1,0:T(8,128)(2,1)}, u32[]{:S(2)}) copy-start(bf16[768,1536]{1,0:T(8,128)(2,1)} %param.31) | copy-start | bytes 7077892
  6.5 81.9 %all-gather.11.cloned.1.call-start = ((), (), s32[]{:S(2)}) async-start(), calls=%async_computation.1 | async-start | bytes 4456448 | tf_op jit(solution)/shard_map/all_gather | solution.py:105
  7.3 158.2 %all-gather.15.cloned.1.call-start = ((), (), s32[]{:S(2)}) async-start(), calls=%async_computation.3 | async-start | bytes 4456448 | tf_op jit(solution)/shard_map/all_gather | solution.py:104
  8.0 234.4 %all-gather.13.cloned.1.call-start = ((), (), s32[]{:S(2)}) async-start(), calls=%async_computation.2 | async-start | bytes 4456448 | tf_op jit(solution)/shard_map/all_gather | solution.py:103
  8.7 306.1 %all-gather.19.cloned.1.call-start = ((), (), s32[]{:S(2)}) async-start(), calls=%async_computation.5 | async-start | bytes 1114112 | tf_op jit(solution)/shard_map/all_gather | solution.py:107
  9.3 349.7 %all-gather.21.cloned.1.call-start = ((), (), s32[]{:S(2)}) async-start(), calls=%async_computation.6 | async-start | bytes 1671168 | tf_op jit(solution)/shard_map/all_gather | solution.py:106
  9.9 394.9 %all-gather.25.cloned.1.call-start = ((), (), s32[]{:S(2)}) async-start(), calls=%async_computation.9 | async-start | bytes 2621440 | tf_op jit(solution)/shard_map/all_gather | solution.py:21
  242.4 6.6 %copy-start.6 = (bf16[1,128,2048]{2,1,0:T(8,128)(2,1)S(1)}, bf16[1,128,2048]{2,1,0:T(8,128)(2,1)}, u32[]{:S(2)}) copy-start(bf16[1,128,2048]{2,1,0:T(8,128)(2,1)} %param.23) | copy-start | bytes 1572868
  242.4 6.6 %copy-start.12 = (f32[2048]{0:T(1024)S(1)}, f32[2048]{0:T(1024)}, u32[]{:S(2)}) copy-start(f32[2048]{0:T(1024)} %param.24) | copy-start | bytes 24580
  249.0 3.9 copy-start.4
  252.9 2.4 copy-start.3
  254.4 7.0 %copy-start.18 = (u32[32]{0:T(128)S(1)}, u32[32]{0:T(128)}, u32[]{:S(2)}) copy-start(u32[32]{0:T(128)} %constant.110) | copy-start | bytes 388
  255.3 1.6 copy-start.9
  255.3 18.5 %copy-start.16 = (f32[1024]{0:T(1024)S(1)}, f32[1024]{0:T(1024)}, u32[]{:S(2)}) copy-start(f32[1024]{0:T(1024)} %param.36) | copy-start | bytes 12292
  255.3 18.6 %copy-start.13 = (bf16[128,64]{0,1:T(8,128)(2,1)S(1)}, bf16[128,64]{0,1:T(8,128)(2,1)}, u32[]{:S(2)}) copy-start(bf16[128,64]{0,1:T(8,128)(2,1)} %param.30) | copy-start | bytes 49156
  255.3 59.4 %copy-start.17 = (f32[512]{0:T(512)S(1)}, f32[512]{0:T(512)}, u32[]{:S(2)}) copy-start(f32[512]{0:T(512)} %param.34) | copy-start | bytes 6148
  259.1 222.9 %all-gather.17.cloned.1.call-start = ((), (), s32[]{:S(2)}) async-start(), calls=%async_computation.4 | async-start | bytes 4456448 | tf_op jit(solution)/shard_map/all_gather | solution.py:109
  259.8 299.2 %all-gather.23.cloned.1.call-start = ((), (), s32[]{:S(2)}) async-start(), calls=%async_computation.7 | async-start | bytes 4456448 | tf_op jit(solution)/shard_map/all_gather | solution.py:110
  260.6 309.7 %reduce-scatter.2.cloned.1.call-start = ((), (), s32[]{:S(2)}) async-start(), calls=%async_computation.8 | async-start | bytes 786432 | tf_op jit(solution)/shard_map/reduce_scatter | solution.py:266
  314.8 48.5 %copy-start.15 = (f32[768]{0:T(1024)S(1)}, f32[768]{0:T(1024)}, u32[]{:S(2)}) copy-start(f32[768]{0:T(1024)} %param.33) | copy-start | bytes 9220
  369.8 2.4 copy-start.5
  369.8 3.9 copy-start.1
  404.8 11.2 %copy-start.11 = (bf16[128,4,128]{2,0,1:T(8,128)(2,1)S(1)}, bf16[128,4,128]{2,0,1:T(8,128)(2,1)}, u32[]{:S(2)}) copy-start(bf16[128,4,128]{2,0,1:T(8,128)(2,1)} %get-tuple-element.310) | copy-start | bytes 393220
  404.8 11.2 %copy-start.14 = (f32[128,4]{0,1:T(4,128)S(1)}, f32[128,4]{0,1:T(4,128)}, u32[]{:S(2)}) copy-start(f32[128,4]{0,1:T(4,128)} %get-tuple-element.314) | copy-start | bytes 6148
  (4 other events, 4.0 us)
Sparse Core Ops, SparseCore 0:
  10.1 78.3 all-gather.10
  91.2 74.1 all-gather.14
  168.2 74.1 all-gather.12
  245.1 54.7 all-gather.18
  302.4 56.5 all-gather.20
  360.4 44.3 all-gather.24
  407.6 74.3 all-gather.16
  484.8 74.1 all-gather.22
  563.7 6.5 reduce-scatter.1
where the time goes:
time: 578 us; the launch traced here: 577 us
  waiting for transfers between devices  402 us (70%)
  blocking collectives  73.4 us (13%)
  local copies, waits for them, and re-layouts  33.6 us (6%)
  matrix products  32.1 us (6%)
  other arithmetic  21 us (4%)
  between operations  14.2 us (2%)
    all_gather x1, waiting for transfers between devices, per_device(): lax.all_gather(w_ret_value, ('sp', 'fs'), axis=0, tiled=True)  75.1 us
    all_gather x1, waiting for transfers between devices, per_device(): lax.all_gather(w_att_out, ('sp', 'fs'), axis=0, tiled=True)  73.2 us
    all_gather x1, waiting for transfers between devices, per_device(): lax.all_gather(w_ret_key, ('sp', 'fs'), axis=0, tiled=True)  70.5 us
    all_gather x1, waiting for transfers between devices, per_device(): lax.all_gather(w_ret_query, ('sp', 'fs'), axis=0, tiled=True)  70.4 us
    all_gather x1, waiting for transfers between devices, per_device(): lax.all_gather(w_ret_out, ('sp', 'fs'), axis=0, tiled=True)  62.4 us
    all_gather x1, blocking collectives, per_device(): lax.all_gather(w_rope_key, ('sp', 'fs'), axis=0, tiled=True)  39.1 us
    all_gather x1, waiting for transfers between devices, prefix(): lax.all_gather(part.astype(kind), axis)  22.3 us
    dot_general x3, local copies, waits for them, and re-layouts, project(): return jnp.dot(normed, weight, preferred_element_type=jnp.float32)  19.6 us
  transfers between devices with their start and end apart: 9, of which 8 were waited for; matrix products, arithmetic and copies ran while one was open for 14% of the time, Pallas kernels for 0%

commit v1 on v0

--- a/solution.py
+++ b/solution.py
@@ -1,6 +1,10 @@
+import functools
+
 import jax
 import jax.numpy as jnp
 from jax import lax
+from jax.experimental import pallas as pl
+from jax.experimental.pallas import tpu as pltpu
 from jax.sharding import PartitionSpec as P
 
 RET_DIM = 256
@@ -64,7 +68,7 @@
     return (early_log + late_log, jnp.exp(late_log)[:, None, None] * early_state + late_state)
 
 
-def per_device(
+def rows_plan(
     tokens,
     norm_gain,
     w_ret_query,
@@ -275,6 +279,379 @@
     return mixed[None]
 
 
+MESH = pl.DeviceIdType.MESH
+
+
+def heads_fit(mesh, ret_local, sequences):
+    sizes = mesh.shape
+    return (
+        sizes["fs"] == 4 and sizes["tp"] == 2 and ret_local == sizes["sp"] and sequences == 1
+    )
+
+
+def gather_kernel(
+    n_sp,
+    tok_ref,
+    lat_ref,
+    wq_ref,
+    wk_ref,
+    wv_ref,
+    wr_ref,
+    wa_ref,
+    shift_ref,
+    tok_all,
+    w_all,
+    shift_all,
+    local_sem,
+    z_send,
+    z_recv,
+    x_send,
+    x_recv,
+    y_send,
+    y_recv,
+    xf_send,
+    xf_recv,
+    yf_send,
+    yf_recv,
+    t_send,
+    t_recv,
+    p_send,
+    p_recv,
+    s_send,
+    s_recv,
+):
+    z, f, t = lax.axis_index("sp"), lax.axis_index("fs"), lax.axis_index("tp")
+    xn = f + 1 - 2 * (f % 2)
+    yn = (f + 2) % 4
+    other = 1 - t
+    rows = tok_ref.shape[0]
+    half = rows // 2
+    wide = lat_ref.shape[2]
+    group = 3 * wide
+    fs = 4
+    weights = (lat_ref, wq_ref, wk_ref, wv_ref, wr_ref, wa_ref)
+
+    def remote(src, dst, send, recv, **where):
+        return pltpu.make_async_remote_copy(
+            src_ref=src,
+            dst_ref=dst,
+            send_sem=send,
+            recv_sem=recv,
+            device_id={"sp": z, "fs": f, "tp": t, **where},
+            device_id_type=MESH,
+        )
+
+    barrier = pltpu.get_barrier_semaphore()
+    peers = [{"sp": (z + d) % n_sp, "fs": f, "tp": t} for d in range(1, n_sp)]
+    peers += [{"sp": z, "fs": xn, "tp": t}, {"sp": z, "fs": yn, "tp": t}]
+    peers += [{"sp": z, "fs": f, "tp": other}]
+    for peer in peers:
+        pl.semaphore_signal(barrier, inc=1, device_id=peer, device_id_type=MESH)
+    pl.semaphore_wait(barrier, len(peers))
+
+    def piece(u, owner):
+        if u == 0:
+            return lat_ref.at[owner]
+        return weights[u].at[:, pl.ds(pl.multiple_of(owner * wide, wide), wide)]
+
+    def block(owner):
+        return pl.ds(pl.multiple_of((owner * fs + f) * rows, rows), rows)
+
+    pending = []
+    mine = pl.ds(pl.multiple_of(t * half, half), half)
+    tok_copies = {}
+    for d in range(1, n_sp):
+        copy = remote(
+            tok_ref.at[mine],
+            tok_all.at[z, mine],
+            t_send.at[d],
+            t_recv.at[d],
+            sp=(z + d) % n_sp,
+        )
+        copy.start()
+        tok_copies[d] = copy
+        copy = remote(
+            shift_ref, shift_all.at[z], s_send.at[d], s_recv.at[d], sp=(z + d) % n_sp
+        )
+        copy.start()
+        pending.append(copy)
+    locals_ = []
+    for u in range(6):
+        copy = pltpu.make_async_copy(
+            piece(u, z), w_all.at[block(z), pl.ds(u * wide, wide)], local_sem.at[u]
+        )
+        copy.start()
+        locals_.append(copy)
+    own_tok = pltpu.make_async_copy(tok_ref, tok_all.at[z], local_sem.at[6])
+    own_tok.start()
+    own_shift = pltpu.make_async_copy(shift_ref, shift_all.at[z], local_sem.at[7])
+    own_shift.start()
+    z_copies = {}
+    for g in range(2):
+        for d in range(1, n_sp):
+            for u in range(3 * g, 3 * g + 3):
+                copy = remote(
+                    piece(u, (z + d) % n_sp),
+                    w_all.at[block(z), pl.ds(u * wide, wide)],
+                    z_send.at[d, u],
+                    z_recv.at[d, u],
+                    sp=(z + d) % n_sp,
+                )
+                copy.start()
+                z_copies[d, u] = copy
+
+    def part(owner_z, owner_f, g):
+        start = pl.multiple_of((owner_z * fs + owner_f) * rows, rows)
+        return w_all.at[pl.ds(start, rows), pl.ds(g * group, group)]
+
+    x_copies, y_copies = {}, {}
+    for d in range(n_sp):
+        owner = (z + n_sp - d) % n_sp
+        for g in range(2):
+            for u in range(3 * g, 3 * g + 3):
+                if d == 0:
+                    locals_[u].wait()
+                else:
+                    z_copies[d, u].wait_recv()
+            ref = part(owner, f, g)
+            x_copies[d, g] = remote(ref, ref, x_send.at[d, g], x_recv.at[d, g], fs=xn)
+            y_copies[d, g] = remote(ref, ref, y_send.at[d, g], y_recv.at[d, g], fs=yn)
+            x_copies[d, g].start()
+            y_copies[d, g].start()
+
+    for d in range(1, n_sp):
+        owner = (z + n_sp - d) % n_sp
+        tok_copies[d].wait_recv()
+        ref = tok_all.at[owner, mine]
+        copy = remote(ref, ref, p_send.at[d], p_recv.at[d], tp=other)
+        copy.start()
+        pending.append(copy)
+
+    for d in range(n_sp):
+        owner = (z + n_sp - d) % n_sp
+        x_copies[d, 0].wait_recv()
+        ref = part(owner, xn, 0)
+        copy = remote(ref, ref, yf_send.at[d], yf_recv.at[d], fs=yn)
+        copy.start()
+        pending.append(copy)
+        y_copies[d, 1].wait_recv()
+        ref = part(owner, yn, 1)
+        copy = remote(ref, ref, xf_send.at[d], xf_recv.at[d], fs=xn)
+        copy.start()
+        pending.append(copy)
+
+    for d in range(n_sp):
+        x_copies[d, 1].wait_recv()
+        y_copies[d, 0].wait_recv()
+    for copy in pending:
+        copy.wait()
+    for d in range(1, n_sp):
+        tok_copies[d].wait_send()
+    for copy in list(z_copies.values()) + list(x_copies.values()) + list(y_copies.values()):
+        copy.wait_send()
+    own_tok.wait()
+    own_shift.wait()
+
+
+def gather_all(n_sp, tokens, lat, wq, wk, wv, wr, wa, shift):
+    rows, width = tokens.shape
+    dma = pltpu.SemaphoreType.DMA
+    return pl.pallas_call(
+        functools.partial(gather_kernel, n_sp),
+        out_shape=(
+            jax.ShapeDtypeStruct((n_sp, rows, width), tokens.dtype),
+            jax.ShapeDtypeStruct((n_sp * 4 * rows, 6 * lat.shape[2]), lat.dtype),
+            jax.ShapeDtypeStruct((n_sp,) + shift.shape, shift.dtype),
+        ),
+        in_specs=[pl.BlockSpec(memory_space=pl.ANY)] * 8,
+        out_specs=(pl.BlockSpec(memory_space=pl.ANY),) * 3,
+        scratch_shapes=[
+            dma((8,)),
+            dma((n_sp, 6)),
+            dma((n_sp, 6)),
+            dma((n_sp, 2)),
+            dma((n_sp, 2)),
+            dma((n_sp, 2)),
+            dma((n_sp, 2)),
+            dma((n_sp,)),
+            dma((n_sp,)),
+            dma((n_sp,)),
+            dma((n_sp,)),
+            dma((n_sp,)),
+            dma((n_sp,)),
+            dma((n_sp,)),
+            dma((n_sp,)),
+            dma((n_sp,)),
+            dma((n_sp,)),
+        ],
+        compiler_params=pltpu.CompilerParams(collective_id=0, has_side_effects=True),
+    )(tokens, lat, wq, wk, wv, wr, wa, shift)
+
+
+def heads_plan(
+    tokens,
+    norm_gain,
+    w_ret_query,
+    w_ret_key,
+    w_ret_value,
+    w_q_down,
+    w_kv_down,
+    w_rope_key,
+    w_q_up,
+    w_kv_up,
+    q_lat_gain,
+    kv_lat_gain,
+    att_norm_gain,
+    ret_norm_gain,
+    w_ret_out,
+    w_att_out,
+    head_rate,
+    decay_shift,
+    start_state,
+):
+    n_sp, n_tp = lax.axis_size("sp"), lax.axis_size("tp")
+    z = lax.axis_index("sp")
+    rows = tokens.shape[1]
+    length = n_sp * rows
+    q_part = w_q_down.shape[1] // n_sp
+    kv_part = w_kv_down.shape[1] // n_sp
+    rope_half = ROPE_DIM // 2
+    rope_part = rope_half // n_sp
+    att_heads = w_q_up.shape[1] // (NOPE_DIM + ROPE_DIM) // n_sp
+    w_rows = w_q_down.shape[0]
+    lat = jnp.concatenate(
+        [
+            w_q_down.reshape(w_rows, n_sp, q_part),
+            w_kv_down.reshape(w_rows, n_sp, kv_part),
+            w_rope_key.reshape(w_rows, 2, n_sp, rope_part)
+            .transpose(0, 2, 1, 3)
+            .reshape(w_rows, n_sp, 2 * rope_part),
+        ],
+        axis=2,
+    ).transpose(1, 0, 2)
+    lat = jnp.pad(lat, ((0, 0), (0, 0), (0, RET_DIM - lat.shape[2])))
+    tok_all, w_all, shift_all = gather_all(
+        n_sp,
+        tokens[0],
+        lat,
+        w_ret_query,
+        w_ret_key,
+        w_ret_value,
+        w_ret_out,
+        w_att_out,
+        decay_shift[0],
+    )
+    positions = jnp.arange(length, dtype=jnp.int32)
+    ret_cos, ret_sin = angle_tables(positions, RET_DIM)
+    rope_cos, rope_sin = angle_tables(positions, ROPE_DIM)
+    source = tok_all.reshape(length, -1).astype(jnp.float32)
+    normed = rms_scale(source, norm_gain).astype(jnp.bfloat16)
+    projected = jnp.dot(normed, w_all[:, : 4 * RET_DIM], preferred_element_type=jnp.float32)
+    rope_at = q_part + kv_part
+    cos_part = lax.dynamic_slice_in_dim(rope_cos, z * rope_part, rope_part, 1)
+    sin_part = lax.dynamic_slice_in_dim(rope_sin, z * rope_part, rope_part, 1)
+    sent = jnp.concatenate(
+        [
+            projected[:, :rope_at],
+            rotate(projected[:, rope_at : rope_at + 2 * rope_part], cos_part, sin_part),
+        ],
+        axis=1,
+    ).astype(jnp.bfloat16)
+    lats = lax.all_gather(sent, ("tp", "sp"), axis=0)
+    lat_q_raw = lats[:, :, :q_part].transpose(1, 0, 2).reshape(length, -1)
+    lat_kv_raw = lats[:, :, q_part:rope_at].transpose(1, 0, 2).reshape(length, -1)
+    rope_key = (
+        lats[:n_sp, :, rope_at:]
+        .reshape(n_sp, length, 2, rope_part)
+        .transpose(1, 2, 0, 3)
+        .reshape(length, ROPE_DIM)
+    )
+
+    ret_q = rotate(projected[:, RET_DIM : 2 * RET_DIM], ret_cos, ret_sin).astype(jnp.bfloat16)
+    ret_k = (
+        rotate(projected[:, 2 * RET_DIM : 3 * RET_DIM], ret_cos, ret_sin) * RET_DIM ** (-0.5)
+    ).astype(jnp.bfloat16)
+    ret_v = projected[:, 3 * RET_DIM : 4 * RET_DIM].astype(jnp.bfloat16)
+    rate = lax.dynamic_index_in_dim(head_rate, z, 0, keepdims=False)
+    shift = lax.dynamic_index_in_dim(shift_all, z, 1, keepdims=False)
+    cumul = jnp.cumsum(rate + shift, axis=1)
+    last = cumul[:, -1]
+    offsets = jnp.arange(rows, dtype=jnp.int32)
+    lower = offsets[None, :] <= offsets[:, None]
+    decay = jnp.exp(jnp.where(lower[None], cumul[:, :, None] - cumul[:, None, :], -jnp.inf))
+    bq, bk, bv = (a.reshape(n_sp, rows, RET_DIM) for a in (ret_q, ret_k, ret_v))
+    scores = (
+        jnp.einsum("bnd,bmd->bnm", bq, bk, preferred_element_type=jnp.float32) * decay
+    ).astype(jnp.bfloat16)
+    inside = jnp.einsum("bnm,bme->bne", scores, bv, preferred_element_type=jnp.float32)
+    weighted = bk.astype(jnp.float32) * jnp.exp(last[:, None] - cumul)[:, :, None]
+    added = jnp.einsum(
+        "bmd,bme->bde", weighted, bv.astype(jnp.float32), precision=TOP_PRECISION
+    )
+    state = lax.dynamic_index_in_dim(start_state[0], z, 0, keepdims=False)
+    states = []
+    for b in range(n_sp):
+        states.append(state)
+        state = jnp.exp(last[b]) * state + added[b]
+    carried = (
+        jnp.einsum(
+            "bnd,bde->bne", bq.astype(jnp.float32), jnp.stack(states), precision=TOP_PRECISION
+        )
+        * jnp.exp(cumul)[:, :, None]
+    )
+    ret_raw = (inside + carried).reshape(length, RET_DIM)
+    row_mean = jnp.mean(ret_raw, axis=-1, keepdims=True)
+    centered = ret_raw - row_mean
+    row_var = jnp.mean(centered * centered, axis=-1, keepdims=True)
+    ret_gain = lax.dynamic_slice_in_dim(ret_norm_gain, z * RET_DIM, RET_DIM, 0)
+    ret_out = (centered * lax.rsqrt(row_var + EPSILON) * ret_gain).astype(jnp.bfloat16)
+
+    q_latent = rms_scale(lat_q_raw.astype(jnp.float32), q_lat_gain).astype(jnp.bfloat16)
+    kv_latent = rms_scale(lat_kv_raw.astype(jnp.float32), kv_lat_gain).astype(jnp.bfloat16)
+    q_wide = att_heads * (NOPE_DIM + ROPE_DIM)
+    kv_wide = att_heads * (NOPE_DIM + VAL_DIM)
+    q_up = lax.dynamic_slice_in_dim(w_q_up, z * q_wide, q_wide, 1)
+    kv_up = lax.dynamic_slice_in_dim(w_kv_up, z * kv_wide, kv_wide, 1)
+    query = jnp.dot(q_latent, q_up, preferred_element_type=jnp.float32)
+    expanded = jnp.dot(kv_latent, kv_up, preferred_element_type=jnp.float32).astype(jnp.bfloat16)
+    att_gain = lax.dynamic_slice_in_dim(
+        att_norm_gain, z * att_heads * VAL_DIM, att_heads * VAL_DIM, 0
+    )
+    allowed = positions[None, :] <= positions[:, None]
+    outs = [ret_out]
+    for h in range(att_heads):
+        q_h = query[:, h * (NOPE_DIM + ROPE_DIM) : (h + 1) * (NOPE_DIM + ROPE_DIM)]
+        q_h = jnp.concatenate(
+            [q_h[:, :NOPE_DIM], rotate(q_h[:, NOPE_DIM:], rope_cos, rope_sin)], axis=1
+        ).astype(jnp.bfloat16)
+        kv_h = expanded[:, h * (NOPE_DIM + VAL_DIM) : (h + 1) * (NOPE_DIM + VAL_DIM)]
+        k_h = jnp.concatenate([kv_h[:, :NOPE_DIM], rope_key], axis=1)
+        s = lax.dot_general(
+            q_h, k_h, (((1,), (1,)), ((), ())), preferred_element_type=jnp.float32
+        ) * (NOPE_DIM + ROPE_DIM) ** (-0.5)
+        s = jnp.where(allowed, s, -jnp.inf)
+        p = jnp.exp(s - jnp.max(s, axis=-1, keepdims=True))
+        total = jnp.sum(p, axis=-1, keepdims=True)
+        raw = (
+            jnp.dot(
+                p.astype(jnp.bfloat16), kv_h[:, NOPE_DIM:], preferred_element_type=jnp.float32
+            )
+            / total
+        )
+        outs.append(
+            rms_scale(raw, att_gain[h * VAL_DIM : (h + 1) * VAL_DIM]).astype(jnp.bfloat16)
+        )
+    merged = jnp.concatenate(outs, axis=1)
+    partial_sum = lax.dot_general(
+        merged,
+        w_all[:, 4 * RET_DIM :],
+        (((1,), (1,)), ((), ())),
+        preferred_element_type=jnp.float32,
+    ).astype(jnp.bfloat16)
+    mixed = lax.psum_scatter(partial_sum, ("sp", "tp"), scatter_dimension=0, tiled=True)
+    return mixed[None]
+
+
 def solution(mesh):
     placed = (
         P("fs", "sp", None),
@@ -297,8 +674,14 @@
         P("fs", "tp", "sp"),
         P("fs", "tp", None, None),
     )
+
+    def pick(*args):
+        if heads_fit(mesh, args[16].shape[0], args[0].shape[0]):
+            return heads_plan(*args)
+        return rows_plan(*args)
+
     return jax.shard_map(
-        per_device,
+        pick,
         mesh=mesh,
         in_specs=placed,
         out_specs=P("fs", ("sp", "tp"), None),

time: 578 us -> 202 us (0.35)
  waiting for transfers between devices: 402 us -> 52.1 us
  Pallas kernels: 0 us -> 91.2 us
  blocking collectives: 73.4 us -> 0 us
  local copies, waits for them, and re-layouts: 33.6 us -> 12.7 us
  matrix products: 32.1 us -> 15.7 us
  other arithmetic: 21 us -> 13.9 us
    all_gather x8 -> x1, waiting for transfers between devices: 391 us -> 16.4 us  [heads_plan(): lats = lax.all_gather(sent, ('tp', 'sp'), axis=0)]
    pallas_call x0 -> x1, Pallas kernels: none -> 91.2 us  [gather_all(): pl.pallas_call(functools.partial(gather_kernel, n_sp), out_shape=(jax.Sha...]
    all_gather x5 -> x0, blocking collectives: 63.1 us -> none  [the longest x1 39.1 us: per_device(): lax.all_gather(w_rope_key, ('sp', 'fs'), axis=0, tiled=True)]
    reduce_scatter x1, waiting for transfers between devices: 6.68 us -> 35.7 us  [heads_plan(): lax.psum_scatter(partial_sum, ('sp', 'tp'), scatter_dimension=0, tiled=True)]
    dot_general x3 -> x0, local copies, waits for them, and re-layouts: 19.6 us -> none  [project(): return jnp.dot(normed, weight, preferred_element_type=jnp.float32)]
    dot_general x16 -> x11, matrix products: 32.1 us -> 15.7 us  [the longest x1 4.55 us: heads_plan(): jnp.dot(normed, w_all[:, :4 * RET_DIM], preferred_element_type=jnp.float32)]
    unnamed x1 -> x0, blocking collectives: 10.3 us -> none
  transfers between devices with their start and end apart: 9 -> 2, of which waited for: 8 -> 2; matrix products, arithmetic and copies ran while one was open for 14% -> 6% of each run, Pallas kernels for 0% -> 0%
where the time goes in v1:
time: 202 us
  Pallas kernels  91.2 us (45%)
  waiting for transfers between devices  52.1 us (26%)
  between operations  15.8 us (8%)
  matrix products  15.7 us (8%)
  other arithmetic  13.9 us (7%)
  local copies, waits for them, and re-layouts  12.7 us (6%)
    pallas_call x1, Pallas kernels, gather_all(): pl.pallas_call(functools.partial(gather_kernel, n_sp), out_shape=(jax.Sha...  91.2 us
    reduce_scatter x1, waiting for transfers between devices, heads_plan(): lax.psum_scatter(partial_sum, ('sp', 'tp'), scatter_dimension=0, tiled=True)  35.7 us
    all_gather x1, waiting for transfers between devices, heads_plan(): lats = lax.all_gather(sent, ('tp', 'sp'), axis=0)  16.4 us
    reduce_sum x3, other arithmetic, rms_scale(): jnp.mean(values * values, axis=-1, keepdims=True) + EPSILON  4.88 us
    dot_general x1, matrix products, heads_plan(): jnp.dot(normed, w_all[:, :4 * RET_DIM], preferred_element_type=jnp.float32)  4.55 us
    dot_general x1, matrix products, heads_plan(): lax.dot_general(merged, w_all[:, 4 * RET_DIM:], (((1,), (1,)), ((), ())),...  4.23 us
  transfers between devices with their start and end apart: 2, of which 2 were waited for; matrix products, arithmetic and copies ran while one was open for 6% of the time, Pallas kernels for 0%

profile of v1, /device:TPU:0, one launch (start us, length us, event | category | flops | bytes accessed | tf_op | source)
XLA Modules:
  0.0 201.7 jit_solution(3056559068700737346)
XLA Ops:
  6.6 0.9 copy.114
  7.4 0.9 copy.96
  8.5 1.0 copy.95
  10.7 91.2 %shard_map.181 = (bf16[4,128,2048]{2,1,0:T(8,128)(2,1)}, bf16[2048,1536]{1,0:T(8,128)(2,1)}, f32[4,4,128]{2,1,0:T(4,128)}) custom-call(bf16[128,2048]{1,0:T(8,128)(2,1)} %bitcast.84, bf16[4,128,256]{2,1,0:T(8,128)(2,1)} %pad.4.lat_ref, bf16[128,1024]{1,0:T(8,128)(2,1)} %wq_ref.1, bf16[128,1024]{1,0:T(8,128)(2,1)} %wk_ref.1, bf16[128,1024]{1,0:T(8,128)(2,1)} %wv_ref.1, ...), custom_call_target="tpu_custom_call" | custom-call | tf_op jit(solution)/shard_map/pallas_call | solution.py:459
  101.9 2.2 %multiply_reduce_fusion = f32[4,128]{1,0:T(4,128)S(1)} fusion(bf16[4,128,2048]{2,1,0:T(8,128)(2,1)} %get-tuple-element.8), kind=kLoop, calls=%fused_computation.5 | loop fusion | flops 3145216 | bytes 2099200 | tf_op jit(solution)/shard_map/reduce_sum | solution.py:60
  104.7 4.6 %fusion.123 = (bf16[512,1024]{1,0:T(8,128)(2,1)S(1)}, f32[512,1024]{1,0:T(8,128)S(1)}) fusion(bf16[512,2048]{1,0:T(8,128)(2,1)S(1)} %fusion.1, bf16[2048,1536]{1,0:T(8,128)(2,1)} %get-tuple-element.9), kind=kOutput, calls=%fused_computation.173 | convolution fusion | flops 2148007936 | bytes 9437184 | tf_op jit(solution)/shard_map/dot_general | solution.py:549
  109.4 1.3 copy-done.3
  112.0 0.8 copy.106
  113.7 1.3 dynamic-slice_add_fusion
  116.2 1.0 slice.172
  117.2 0.8 dynamic_slice.41
  117.9 0.8 dynamic_slice.36
  120.8 2.3 %fusion.56 = (f32[512,128]{1,0:T(8,128)S(1)}, f32[512,128]{1,0:T(8,128)S(1)}, bf16[512,128]{1,0:T(8,128)(2,1)S(1)}, bf16[512,128]{1,0:T(8,128)(2,1)S(1)}) fusion(f32[512,1024]{1,0:T(8,128)} %copy-done.3, f32[128]{0:T(128)S(1)} %multiply_power_fusion.1, f32[512]{0:T(512)S(1)} %iota_convert_fusion), kind=kLoop, calls=%fused_computation.78 | loop fusion | flops 983040 | bytes 1837568 | tf_op jit(solution)/shard_map/sub | solution.py:53
  123.1 1.2 fusion.11
  125.0 1.0 slice_add_fusion
  127.2 16.4 %all-gather.2.cloned.1.call-done = bf16[8,512,176]{1,2,0:T(8,128)(2,1)} async-done(((bf16[1,512,176]{1,2,0:T(8,128)(2,1)}), bf16[8,512,176]{1,2,0:T(8,128)(2,1)}) %all-gather.2.cloned.1.call-update) | async-done | bytes 1441808 | tf_op jit(solution)/shard_map/all_gather | solution.py:560
  143.6 1.3 multiply_reduce_fusion.2
  145.0 1.4 multiply_reduce_fusion.1
  146.3 0.8 slice_bitcast_fusion.1
  148.2 1.0 fusion.89
  149.5 1.5 convolution_convert_fusion.1
  152.8 1.3 fusion.125
  154.9 4.2 %convolution_convert_fusion = bf16[512,2048]{1,0:T(8,128)(2,1)} fusion(bf16[2048,1536]{1,0:T(8,128)(2,1)} %get-tuple-element.9, bf16[512,128]{1,0:T(8,128)(2,1)S(1)} %copy.109, bf16[512,128]{1,0:T(8,128)(2,1)S(1)} %copy.108, bf16[512,256]{1,0:T(8,128)(2,1)S(1)} %fusion.37), kind=kOutput, calls=%fused_computation.6 | convolution fusion | flops 1076363264 | bytes 4718592 | tf_op jit(solution)/shard_map/dot_general | solution.py:645
  159.2 35.7 %reduce-scatter.2.cloned.1.call-done = bf16[64,2048]{1,0:T(8,128)(2,1)} async-done(((bf16[512,2048]{1,0:T(8,128)(2,1)}), bf16[64,2048]{1,0:T(8,128)(2,1)}) %reduce-scatter.2.cloned.1.call-update) | async-done | bytes 262160 | tf_op jit(solution)/shard_map/reduce_scatter | solution.py:651
  (77 shorter events, 11.0 us)
Async XLA Ops:
  6.5 141.1 %copy-start = (bf16[768,1536]{1,0:T(8,128)(2,1)S(1)}, bf16[768,1536]{1,0:T(8,128)(2,1)}, u32[]{:S(2)}) copy-start(bf16[768,1536]{1,0:T(8,128)(2,1)} %param.27) | copy-start | bytes 7077892
  6.5 137.1 %all-gather.2.cloned.1.call-start = ((), (), s32[]{:S(2)}) async-start(), calls=%async_computation.1 | async-start | bytes 1622016 | tf_op jit(solution)/shard_map/all_gather | solution.py:560
  10.7 93.4 %copy-start.6 = (f32[2048]{0:T(1024)S(1)}, f32[2048]{0:T(1024)}, u32[]{:S(2)}) copy-start(f32[2048]{0:T(1024)} %param.20) | copy-start | bytes 24580
  101.9 2.3 %copy-start.1 = (bf16[4,128,2048]{2,1,0:T(8,128)(2,1)S(1)}, bf16[4,128,2048]{2,1,0:T(8,128)(2,1)}, u32[]{:S(2)}) copy-start(bf16[4,128,2048]{2,1,0:T(8,128)(2,1)} %get-tuple-element.8) | copy-start | bytes 6291460
  109.3 1.3 copy-start.3
  109.3 1.7 copy-start.4
  109.3 3.8 %copy-start.9 = (f32[4]{0:T(128)S(1)}, f32[4]{0:T(128)}, u32[]{:S(2)}) copy-start(f32[4]{0:T(128)} %param.35) | copy-start | bytes 52
  112.8 82.0 %reduce-scatter.2.cloned.1.call-start = ((), (), s32[]{:S(2)}) async-start(), calls=%async_computation.2 | async-start | bytes 2359296 | tf_op jit(solution)/shard_map/reduce_scatter | solution.py:651
  124.3 1.8 copy-start.10
  127.2 20.2 %copy-start.7 = (f32[768]{0:T(1024)S(1)}, f32[768]{0:T(1024)}, u32[]{:S(2)}) copy-start(f32[768]{0:T(1024)} %param.29) | copy-start | bytes 9220
  143.6 3.5 %copy-start.2 = (bf16[8,512,176]{1,2,0:T(8,128)(2,1)S(1)}, bf16[8,512,176]{1,2,0:T(8,128)(2,1)}, u32[]{:S(2)}) copy-start(bf16[8,512,176]{1,2,0:T(8,128)(2,1)} %all-gather.2.cloned.1.call-done) | copy-start | bytes 4325380
  147.2 4.5 %copy-start.5 = (bf16[512,2,4,8]{0,3,2,1:T(8,128)(2,1)}, bf16[512,2,4,8]{0,3,2,1:T(8,128)(2,1)S(1)}, u32[]{:S(2)}) copy-start(bf16[512,2,4,8]{0,3,2,1:T(8,128)(2,1)S(1)} %copy.107) | copy-start | bytes 196612
  147.7 1.6 copy-start.8
Sparse Core Ops, SparseCore 0:
  112.9 30.6 all-gather.1
  159.3 35.5 reduce-scatter.1

commit v2 on v0

--- a/solution.py
+++ b/solution.py
@@ -1,6 +1,10 @@
+import functools
+
 import jax
 import jax.numpy as jnp
 from jax import lax
+from jax.experimental import pallas as pl
+from jax.experimental.pallas import tpu as pltpu
 from jax.sharding import PartitionSpec as P
 
 RET_DIM = 256
@@ -64,7 +68,7 @@
     return (early_log + late_log, jnp.exp(late_log)[:, None, None] * early_state + late_state)
 
 
-def per_device(
+def rows_plan(
     tokens,
     norm_gain,
     w_ret_query,
@@ -275,6 +279,586 @@
     return mixed[None]
 
 
+MESH = pl.DeviceIdType.MESH
+WIDE = RET_DIM
+CONTRACT = (((1,), (1,)), ((), ()))
+GROUPS = ((0, 2), (2, 2), (4, 1), (5, 1))
+FIRST, LATER = (0, 1), (2, 3)
+
+
+def heads_fit(mesh, ret_local, sequences, q_wide, kv_wide):
+    sizes = mesh.shape
+    return (
+        sizes["fs"] == 4
+        and sizes["tp"] == 2
+        and ret_local == sizes["sp"]
+        and sequences == 1
+        and q_wide % 128 == 0
+        and kv_wide % 128 == 0
+        and q_wide + kv_wide + 2 * ROPE_DIM <= ret_local * WIDE
+    )
+
+
+def three_parts(x):
+    high = x.astype(jnp.bfloat16)
+    rest = x - high.astype(jnp.float32)
+    middle = rest.astype(jnp.bfloat16)
+    low = (rest - middle.astype(jnp.float32)).astype(jnp.bfloat16)
+    return high, middle, low
+
+
+def layer_kernel(
+    n_sp,
+    q_wide,
+    kv_wide,
+    tok_ref,
+    lat_ref,
+    wq_ref,
+    wk_ref,
+    wv_ref,
+    wr_ref,
+    wa_ref,
+    shift_ref,
+    rate_ref,
+    gain_ref,
+    qgain_ref,
+    kvgain_ref,
+    again_ref,
+    rgain_ref,
+    rcos_ref,
+    rsin_ref,
+    pcos_ref,
+    psin_ref,
+    qup_ref,
+    kvup_ref,
+    start_ref,
+    out_ref,
+    tok_all,
+    w_all,
+    shift_all,
+    normed,
+    acc,
+    ret_q,
+    ret_k,
+    ret_v,
+    lat_all,
+    state,
+    qn,
+    qr,
+    expanded,
+    rope_key,
+    kvup,
+    merged,
+    own_sum,
+    pair_out,
+    pair_in,
+    row_out,
+    row_in,
+    local_sem,
+    z_send,
+    z_recv,
+    x_send,
+    x_recv,
+    y_send,
+    y_recv,
+    f_send,
+    f_recv,
+    m_send,
+    m_recv,
+):
+    z, f, t = lax.axis_index("sp"), lax.axis_index("fs"), lax.axis_index("tp")
+    xn = f + 1 - 2 * (f % 2)
+    yn = (f + 2) % 4
+    other = 1 - t
+    fs = 4
+    rows = tok_ref.shape[0]
+    half = rows // 2
+    weights = (lat_ref, wq_ref, wk_ref, wv_ref, wr_ref, wa_ref)
+    f32, bf16 = jnp.float32, jnp.bfloat16
+
+    def remote(src, dst, send, recv, **where):
+        return pltpu.make_async_remote_copy(
+            src_ref=src,
+            dst_ref=dst,
+            send_sem=send,
+            recv_sem=recv,
+            device_id={"sp": z, "fs": f, "tp": t, **where},
+            device_id_type=MESH,
+        )
+
+    barrier = pltpu.get_barrier_semaphore()
+    peers = [{"sp": (z + d) % n_sp, "fs": f, "tp": t} for d in range(1, n_sp)]
+    peers += [{"sp": z, "fs": xn, "tp": t}, {"sp": z, "fs": yn, "tp": t}]
+    peers += [{"sp": z, "fs": f, "tp": other}]
+    for peer in peers:
+        pl.semaphore_signal(barrier, inc=1, device_id=peer, device_id_type=MESH)
+    pl.semaphore_wait(barrier, len(peers))
+
+    def piece(u, owner):
+        return weights[u].at[:, pl.ds(pl.multiple_of(owner * WIDE, WIDE), WIDE)]
+
+    def part(owner_z, owner_f, g):
+        first, count = GROUPS[g]
+        start = pl.multiple_of((owner_z * fs + owner_f) * rows, rows)
+        return w_all.at[pl.ds(start, rows), pl.ds(first * WIDE, count * WIDE)]
+
+    def unit(u):
+        start = pl.multiple_of((z * fs + f) * rows, rows)
+        return w_all.at[pl.ds(start, rows), pl.ds(u * WIDE, WIDE)]
+
+    pending = []
+
+    def go(copy):
+        copy.start()
+        pending.append(copy)
+        return copy
+
+    def owner(d):
+        return (z + n_sp - d) % n_sp
+
+    mine = pl.ds(pl.multiple_of(t * half, half), half)
+    tok_copies, z_copies, x_copies, y_copies, f_copies = {}, {}, {}, {}, {}
+    for d in range(1, n_sp):
+        to = (z + d) % n_sp
+        tok_copies[d] = remote(
+            tok_ref.at[mine], tok_all.at[z, mine], m_send.at[0, d], m_recv.at[0, d], sp=to
+        )
+        tok_copies[d].start()
+    for d in range(1, n_sp):
+        to = (z + d) % n_sp
+        go(remote(shift_ref, shift_all.at[z], m_send.at[2, d], m_recv.at[2, d], sp=to))
+    shift_copies = list(pending)
+    pending.clear()
+    locals_ = []
+    for u in range(6):
+        copy = pltpu.make_async_copy(piece(u, z), unit(u), local_sem.at[u])
+        copy.start()
+        locals_.append(copy)
+    own_tok = pltpu.make_async_copy(tok_ref, tok_all.at[z], local_sem.at[6])
+    own_tok.start()
+    own_shift = pltpu.make_async_copy(shift_ref, shift_all.at[z], local_sem.at[7])
+    own_shift.start()
+    att_wide = kvup.shape[1]
+    own_kvup = pltpu.make_async_copy(
+        kvup_ref.at[:, pl.ds(pl.multiple_of(z * att_wide, att_wide), att_wide)],
+        kvup,
+        local_sem.at[8],
+    )
+    own_kvup.start()
+    own_state = pltpu.make_async_copy(start_ref.at[z], state, local_sem.at[9])
+    own_state.start()
+    for group in (FIRST, LATER):
+        for d in range(1, n_sp):
+            to = (z + d) % n_sp
+            for g in group:
+                for u in range(GROUPS[g][0], sum(GROUPS[g])):
+                    z_copies[d, u] = remote(
+                        piece(u, to), unit(u), z_send.at[d, u], z_recv.at[d, u], sp=to
+                    )
+                    z_copies[d, u].start()
+
+    def spread(d, group):
+        for g in group:
+            for u in range(GROUPS[g][0], sum(GROUPS[g])):
+                if d == 0:
+                    locals_[u].wait()
+                else:
+                    z_copies[d, u].wait_recv()
+            ref = part(owner(d), f, g)
+            x_copies[d, g] = remote(ref, ref, x_send.at[d, g], x_recv.at[d, g], fs=xn)
+            y_copies[d, g] = remote(ref, ref, y_send.at[d, g], y_recv.at[d, g], fs=yn)
+            x_copies[d, g].start()
+            y_copies[d, g].start()
+
+    def relay(d, group):
+        for g in group:
+            if g % 2 == 0:
+                x_copies[d, g].wait_recv()
+                ref, to = part(owner(d), xn, g), yn
+            else:
+                y_copies[d, g].wait_recv()
+                ref, to = part(owner(d), yn, g), xn
+            f_copies[d, g] = remote(ref, ref, f_send.at[d, g], f_recv.at[d, g], fs=to)
+            f_copies[d, g].start()
+
+    def arrive(d, group):
+        for g in group:
+            if g % 2 == 0:
+                y_copies[d, g].wait_recv()
+            else:
+                x_copies[d, g].wait_recv()
+            f_copies[d, g].wait_recv()
+
+    def at(i):
+        return pl.ds(pl.multiple_of(i * rows, rows), rows)
+
+    def norm_block(i):
+        x = tok_all[i].astype(f32)
+        scaled = x * lax.rsqrt(jnp.mean(x * x, axis=-1, keepdims=True) + EPSILON)
+        normed[at(i), :] = (scaled * gain_ref[...]).astype(bf16)
+
+    spread(0, FIRST)
+    own_tok.wait()
+    norm_block(z)
+    tok_pair = {}
+    for d in range(1, n_sp):
+        tok_copies[d].wait_recv()
+        ref = tok_all.at[owner(d), mine]
+        tok_pair[d] = go(remote(ref, ref, m_send.at[1, d], m_recv.at[1, d], tp=other))
+    for d in range(1, n_sp):
+        spread(d, FIRST)
+        relay(d - 1, FIRST)
+        tok_pair[d].wait_recv()
+        norm_block(owner(d))
+    relay(n_sp - 1, FIRST)
+    spread(0, LATER)
+    depth = fs * rows
+    for d in range(n_sp):
+        arrive(d, FIRST)
+        begin = pl.multiple_of(owner(d) * depth, depth)
+
+        def multiply(i, carry, d=d, begin=begin):
+            got = jnp.dot(
+                normed[at(i), pl.ds(begin, depth)],
+                w_all[pl.ds(begin, depth), : 4 * WIDE],
+                preferred_element_type=f32,
+            )
+            if d == 0:
+                acc[at(i), :] = got
+            else:
+                acc[at(i), :] += got
+            return carry
+
+        lax.fori_loop(0, n_sp, multiply, 0)
+
+    rope_index = (q_wide + kv_wide) // WIDE
+    rope_lane = (q_wide + kv_wide) % WIDE
+    rd = RET_DIM // 2
+
+    def finish_lat(i, carry):
+        raw = acc[at(i), :WIDE]
+        pair = raw[:, rope_lane : rope_lane + 2 * ROPE_DIM]
+        turned = pair * pcos_ref[at(i), :] + pltpu.roll(pair, ROPE_DIM, 1) * psin_ref[at(i), :]
+        lane = lax.broadcasted_iota(jnp.int32, turned.shape, 1)
+        turned = jnp.where(lane < ROPE_DIM, turned, pltpu.roll(turned, ROPE_DIM, 1))
+        pieces = [raw[:, :rope_lane]] if rope_lane else []
+        pieces.append(jnp.where(z == rope_index, turned, pair))
+        if rope_lane + 2 * ROPE_DIM < WIDE:
+            pieces.append(raw[:, rope_lane + 2 * ROPE_DIM :])
+        lat_all[t, z, at(i), :] = jnp.concatenate(pieces, axis=1).astype(bf16)
+        return carry
+
+    lax.fori_loop(0, n_sp, finish_lat, 0)
+    lat_copies = {}
+    lat_own = lat_all.at[t, z]
+    lat_pair = {0: go(remote(lat_own, lat_own, m_send.at[4, 0], m_recv.at[4, 0], tp=other))}
+    for d in range(1, n_sp):
+        lat_copies[d] = remote(
+            lat_own, lat_own, m_send.at[3, d], m_recv.at[3, d], sp=(z + d) % n_sp
+        )
+        lat_copies[d].start()
+
+    def finish_ret(i, carry):
+        cosine, sine = rcos_ref[at(i), :], rsin_ref[at(i), :]
+        for dst, base, factor in ((ret_q, WIDE, 1.0), (ret_k, 2 * WIDE, RET_DIM ** (-0.5))):
+            a, b = acc[at(i), base : base + rd], acc[at(i), base + rd : base + WIDE]
+            dst[at(i), :rd] = ((a * cosine - b * sine) * factor).astype(bf16)
+            dst[at(i), rd:] = ((b * cosine + a * sine) * factor).astype(bf16)
+        ret_v[at(i), :] = acc[at(i), 3 * WIDE :].astype(bf16)
+        return carry
+
+    lax.fori_loop(0, n_sp, finish_ret, 0)
+
+    for copy in shift_copies:
+        copy.wait()
+    own_shift.wait()
+    own_state.wait()
+    r_iota = lax.broadcasted_iota(jnp.int32, (rows, rows), 0)
+    c_iota = lax.broadcasted_iota(jnp.int32, (rows, rows), 1)
+
+    def retention(b):
+        rates = shift_all[b] + rate_ref[...]
+        pick = lax.broadcasted_iota(jnp.int32, rates.shape, 0) == z
+        row = jnp.sum(jnp.where(pick, rates, 0.0), axis=0, keepdims=True)
+        column = jnp.sum(jnp.where(r_iota == c_iota, row, 0.0), axis=1, keepdims=True)
+        c_col = jnp.sum(jnp.where(c_iota <= r_iota, row, 0.0), axis=1, keepdims=True)
+        c_row = jnp.sum(jnp.where(r_iota <= c_iota, column, 0.0), axis=0, keepdims=True)
+        last = jnp.sum(row, axis=1, keepdims=True)
+        decay = jnp.exp(jnp.where(c_iota <= r_iota, c_col - c_row, -jnp.inf))
+        block = slice(b * rows, (b + 1) * rows)
+        q, k, v = ret_q[block, :], ret_k[block, :], ret_v[block, :]
+        scores = lax.dot_general(q, k, CONTRACT, preferred_element_type=f32) * decay
+        raw = jnp.dot(scores.astype(bf16), v, preferred_element_type=f32)
+        carried = sum(
+            jnp.dot(q, s, preferred_element_type=f32) for s in three_parts(state[...])
+        )
+        raw = raw + carried * jnp.exp(c_col)
+        if b < n_sp - 1:
+            weighted = k.astype(f32) * jnp.exp(last - c_col)
+            added = sum(
+                lax.dot_general(w, v, (((0,), (0,)), ((), ())), preferred_element_type=f32)
+                for w in three_parts(weighted)
+            )
+            state[...] = jnp.exp(last) * state[...] + added
+        centered = raw - jnp.mean(raw, axis=-1, keepdims=True)
+        variance = jnp.mean(centered * centered, axis=-1, keepdims=True)
+        merged[block, :WIDE] = (centered * lax.rsqrt(variance + EPSILON) * rgain_ref[z]).astype(
+            bf16
+        )
+
+    for b in range(n_sp):
+        if b:
+            spread(b, LATER)
+            relay(b - 1, LATER)
+            lat_copies[b].wait_recv()
+            ref = lat_all.at[t, owner(b)]
+            lat_pair[b] = go(remote(ref, ref, m_send.at[4, b], m_recv.at[4, b], tp=other))
+        retention(b)
+    relay(n_sp - 1, LATER)
+    for d in range(n_sp):
+        lat_pair[d].wait_recv()
+    own_kvup.wait()
+
+    def chunks(first, count):
+        found = []
+        for core in range(2):
+            for j in range(count // 128):
+                lane = first + j * 128
+                found.append((core, lane // WIDE, lane % WIDE))
+        return found
+
+    q_chunks, kv_chunks = chunks(0, q_wide), chunks(q_wide, kv_wide)
+    rope_at = (rope_index, rope_lane)
+    att_heads = att_wide // (NOPE_DIM + VAL_DIM)
+    nope = att_heads * NOPE_DIM
+    turn = att_heads * ROPE_DIM
+
+    def expand(i, carry):
+        def latent(found, gain):
+            x = jnp.concatenate(
+                [lat_all[c, s, at(i), lane : lane + 128] for c, s, lane in found], axis=1
+            ).astype(f32)
+            scaled = x * lax.rsqrt(jnp.mean(x * x, axis=-1, keepdims=True) + EPSILON)
+            return (scaled * gain[...]).astype(bf16)
+
+        query = jnp.dot(latent(q_chunks, qgain_ref), qup_ref[...], preferred_element_type=f32)
+        qn[at(i), :] = query[:, :nope].astype(bf16)
+        qr[at(i), :] = (
+            query[:, nope : nope + turn] * pcos_ref[at(i), :]
+            + query[:, nope + turn :] * psin_ref[at(i), :]
+        ).astype(bf16)
+        expanded[at(i), :] = jnp.dot(
+            latent(kv_chunks, kvgain_ref), kvup[...], preferred_element_type=f32
+        ).astype(bf16)
+        rope_key[at(i), :] = lat_all[0, rope_at[0], at(i), rope_at[1] : rope_at[1] + 128]
+        return carry
+
+    lax.fori_loop(0, n_sp, expand, 0)
+    scale = (NOPE_DIM + ROPE_DIM) ** (-0.5)
+    for b in range(n_sp):
+        seen = (b + 1) * rows
+        block = slice(b * rows, seen)
+        q_at = lax.broadcasted_iota(jnp.int32, (rows, seen), 0) + b * rows
+        k_at = lax.broadcasted_iota(jnp.int32, (rows, seen), 1)
+        for h in range(att_heads):
+            base = h * (NOPE_DIM + VAL_DIM)
+            turned = qr[block, :]
+            lane = lax.broadcasted_iota(jnp.int32, turned.shape, 1)
+            turned = jnp.where(lane // ROPE_DIM == h, turned, jnp.zeros_like(turned))
+            s = lax.dot_general(
+                qn[block, h * NOPE_DIM : (h + 1) * NOPE_DIM],
+                expanded[:seen, base : base + NOPE_DIM],
+                CONTRACT,
+                preferred_element_type=f32,
+            ) + lax.dot_general(
+                turned, rope_key[:seen, :], CONTRACT, preferred_element_type=f32
+            )
+            s = jnp.where(k_at <= q_at, s * scale, -jnp.inf)
+            p = jnp.exp(s - jnp.max(s, axis=-1, keepdims=True))
+            raw = jnp.dot(
+                p.astype(bf16),
+                expanded[:seen, base + NOPE_DIM : base + NOPE_DIM + VAL_DIM],
+                preferred_element_type=f32,
+            ) / jnp.sum(p, axis=-1, keepdims=True)
+            scaled = raw * lax.rsqrt(jnp.mean(raw * raw, axis=-1, keepdims=True) + EPSILON)
+            gain = again_ref[z][:, h * VAL_DIM : (h + 1) * VAL_DIM]
+            merged[block, WIDE + h * VAL_DIM : WIDE + (h + 1) * VAL_DIM] = (
+                scaled * gain
+            ).astype(bf16)
+
+    for d in range(n_sp):
+        arrive(d, LATER)
+    theirs = pl.ds(pl.multiple_of(other * half, half), half)
+    pair_copies, row_copies = {}, {}
+    order = list(range(1, n_sp)) + [0]
+    for d in order:
+        target = (z + d) % n_sp
+        start = pl.multiple_of(target * rows, rows)
+        for which in (theirs, mine):
+            got = lax.dot_general(
+                merged[pl.ds(pl.multiple_of(start + which.start, half), half), :],
+                w_all[:, 4 * WIDE :],
+                CONTRACT,
+                preferred_element_type=f32,
+            )
+            if which is theirs:
+                pair_out[d] = got.astype(bf16)
+                pair_copies[d] = remote(
+                    pair_out.at[d], pair_in.at[d], m_send.at[5, d], m_recv.at[5, d], tp=other
+                )
+                pair_copies[d].start()
+            else:
+                own_sum[d] = got
+    for d in order:
+        pair_copies[d].wait_recv()
+        total = own_sum[d] + pair_in[d].astype(f32)
+        if d:
+            row_out[d] = total.astype(bf16)
+            row_copies[d] = remote(
+                row_out.at[d],
+                row_in.at[d],
+                m_send.at[6, d],
+                m_recv.at[6, d],
+                sp=(z + d) % n_sp,
+            )
+            row_copies[d].start()
+        else:
+            own_sum[0] = total
+    total = own_sum[0]
+    for d in range(1, n_sp):
+        row_copies[d].wait_recv()
+        total = total + row_in[d].astype(f32)
+    out_ref[...] = total.astype(bf16)
+
+    sent = pending + [c for group in (
+        tok_copies, z_copies, x_copies, y_copies, f_copies, lat_copies, pair_copies, row_copies
+    ) for c in group.values()]
+    for copy in sent:
+        copy.wait_send()
+
+
+def heads_plan(
+    tokens,
+    norm_gain,
+    w_ret_query,
+    w_ret_key,
+    w_ret_value,
+    w_q_down,
+    w_kv_down,
+    w_rope_key,
+    w_q_up,
+    w_kv_up,
+    q_lat_gain,
+    kv_lat_gain,
+    att_norm_gain,
+    ret_norm_gain,
+    w_ret_out,
+    w_att_out,
+    head_rate,
+    decay_shift,
+    start_state,
+):
+    n_sp = lax.axis_size("sp")
+    z = lax.axis_index("sp")
+    rows, width = tokens.shape[1:]
+    length = n_sp * rows
+    q_wide, kv_wide = w_q_down.shape[1], w_kv_down.shape[1]
+    rope_half = ROPE_DIM // 2
+    w_rows = w_q_down.shape[0]
+    att_heads = w_q_up.shape[1] // (NOPE_DIM + ROPE_DIM) // n_sp
+
+    def swap(x):
+        return jnp.concatenate([x[..., rope_half:], x[..., :rope_half]], axis=-1)
+
+    lat = jnp.concatenate([w_q_down, w_kv_down, w_rope_key, swap(w_rope_key)], axis=1)
+    lat = jnp.pad(lat, ((0, 0), (0, n_sp * WIDE - lat.shape[1])))
+    head_wide = NOPE_DIM + ROPE_DIM
+    q_up = lax.dynamic_slice_in_dim(w_q_up, z * att_heads * head_wide, att_heads * head_wide, 1)
+    q_up = q_up.reshape(-1, att_heads, head_wide)
+    turned = q_up[..., NOPE_DIM:]
+    q_up = jnp.concatenate(
+        [a.reshape(a.shape[0], -1) for a in (q_up[..., :NOPE_DIM], turned, swap(turned))], axis=1
+    )
+    positions = jnp.arange(length, dtype=jnp.int32)
+    ret_cos, ret_sin = angle_tables(positions, RET_DIM)
+    rope_cos, rope_sin = angle_tables(positions, ROPE_DIM)
+    pair_cos = jnp.concatenate([rope_cos] * 4, axis=1)
+    pair_sin = jnp.concatenate([-rope_sin, rope_sin] * 2, axis=1)
+    dma = pltpu.SemaphoreType.DMA
+    vmem = pltpu.VMEM
+    f32, bf16 = jnp.float32, jnp.bfloat16
+    half = rows // 2
+    out_wide = 4 * n_sp * w_rows
+    any_spec = pl.BlockSpec(memory_space=pl.ANY)
+    vmem_spec = pl.BlockSpec(memory_space=pltpu.VMEM)
+    mixed = pl.pallas_call(
+        functools.partial(layer_kernel, n_sp, q_wide, kv_wide),
+        out_shape=jax.ShapeDtypeStruct((half, out_wide), bf16),
+        in_specs=[any_spec] * 8 + [vmem_spec] * 11 + [any_spec] * 2,
+        out_specs=vmem_spec,
+        scratch_shapes=[
+            vmem((n_sp, rows, width), bf16),
+            vmem((n_sp * 4 * w_rows, 6 * WIDE), bf16),
+            vmem((n_sp,) + decay_shift.shape[1:], f32),
+            vmem((length, width), bf16),
+            vmem((length, 4 * WIDE), f32),
+            vmem((length, WIDE), bf16),
+            vmem((length, WIDE), bf16),
+            vmem((length, WIDE), bf16),
+            vmem((2, n_sp, length, WIDE), bf16),
+            vmem((RET_DIM, RET_DIM), f32),
+            vmem((length, att_heads * NOPE_DIM), bf16),
+            vmem((length, att_heads * ROPE_DIM), bf16),
+            vmem((length, att_heads * (NOPE_DIM + VAL_DIM)), bf16),
+            vmem((length, 2 * ROPE_DIM), bf16),
+            vmem((w_kv_up.shape[0], att_heads * (NOPE_DIM + VAL_DIM)), bf16),
+            vmem((length, WIDE + att_heads * VAL_DIM), bf16),
+            vmem((n_sp, half, out_wide), f32),
+            vmem((n_sp, half, out_wide), bf16),
+            vmem((n_sp, half, out_wide), bf16),
+            vmem((n_sp, half, out_wide), bf16),
+            vmem((n_sp, half, out_wide), bf16),
+            dma((10,)),
+            dma((n_sp, 6)),
+            dma((n_sp, 6)),
+            dma((n_sp, 4)),
+            dma((n_sp, 4)),
+            dma((n_sp, 4)),
+            dma((n_sp, 4)),
+            dma((n_sp, 4)),
+            dma((n_sp, 4)),
+            dma((7, n_sp)),
+            dma((7, n_sp)),
+        ],
+        compiler_params=pltpu.CompilerParams(
+            collective_id=0, has_side_effects=True, vmem_limit_bytes=62 * 1024 * 1024
+        ),
+    )(
+        tokens[0],
+        lat,
+        w_ret_query,
+        w_ret_key,
+        w_ret_value,
+        w_ret_out,
+        w_att_out,
+        decay_shift[0],
+        head_rate[:, None],
+        norm_gain[None],
+        q_lat_gain[None],
+        kv_lat_gain[None],
+        att_norm_gain.reshape(n_sp, 1, -1),
+        ret_norm_gain.reshape(n_sp, 1, -1),
+        ret_cos,
+        ret_sin,
+        pair_cos,
+        pair_sin,
+        q_up,
+        w_kv_up,
+        start_state[0],
+    )
+    return mixed[None]
+
+
 def solution(mesh):
     placed = (
         P("fs", "sp", None),
@@ -297,8 +881,16 @@
         P("fs", "tp", "sp"),
         P("fs", "tp", None, None),
     )
+
+    def pick(*args):
+        if heads_fit(
+            mesh, args[16].shape[0], args[0].shape[0], args[5].shape[1], args[6].shape[1]
+        ):
+            return heads_plan(*args)
+        return rows_plan(*args)
+
     return jax.shard_map(
-        per_device,
+        pick,
         mesh=mesh,
         in_specs=placed,
         out_specs=P("fs", ("sp", "tp"), None),

time: 578 us -> 152 us (0.26)
  the two profiles are of different devices: /device:TPU:0 before, /device:TPU:27 now
where the time goes in v2:
time: 152 us
  Pallas kernels  140 us (92%)
  local copies, waits for them, and re-layouts  5.94 us (4%)
  other arithmetic  5.28 us (3%)
    pallas_call x1, Pallas kernels, heads_plan(): pl.pallas_call(functools.partial(layer_kernel, n_sp, q_wide, kv_wide), ou...  140 us

profile of v2, /device:TPU:27, one launch (start us, length us, event | category | flops | bytes accessed | tf_op | source)
XLA Modules:
  0.0 151.5 jit_solution(9772925241487900841)
XLA Ops:
  0.0 1.1 constant_dynamic-slice_fusion
  1.1 0.3 copy.42
  1.4 0.2 copy.39
  1.6 0.2 copy.41
  1.8 0.2 copy.38
  2.0 0.0 copy-start.2
  2.0 0.0 copy-start
  2.0 0.0 copy-start.1
  2.0 1.0 pad_maximum_fusion.qup_ref
  3.0 1.0 fusion
  4.0 0.0 copy-start.3
  4.0 0.0 copy-start.4
  4.0 1.3 pad_maximum_fusion.1
  5.3 0.1 copy.34
  5.4 0.1 fusion.2
  5.5 0.0 copy-done
  5.5 0.1 concatenate.15
  5.6 0.7 pad.4.lat_ref
  6.4 2.0 %multiply_sine_fusion.1 = (f32[512,128]{1,0:T(8,128)}, f32[512,128]{1,0:T(8,128)}) fusion(f32[128]{0:T(128)S(1)} %multiply_power_fusion.1, f32[512]{0:T(512)S(1)} %iota_convert_fusion), kind=kLoop, calls=%fused_computation.3 | loop fusion | flops 65536 | bytes 526848 | tf_op jit(solution)/shard_map/sin | solution.py:45
  8.4 0.0 copy-done.3
  8.4 0.6 broadcast_in_dim.21.qgain_ref
  9.0 0.7 copy.40.rate_ref
  9.7 140.2 %shard_map.181 = bf16[64,2048]{1,0:T(8,128)(2,1)} custom-call(bf16[128,2048]{1,0:T(8,128)(2,1)} %bitcast.21, bf16[128,1024]{1,0:T(8,128)(2,1)} %pad.4.lat_ref, bf16[128,1024]{1,0:T(8,128)(2,1)} %wq_ref.1, bf16[128,1024]{1,0:T(8,128)(2,1)} %wk_ref.1, bf16[128,1024]{1,0:T(8,128)(2,1)} %wv_ref.1, bf16[128,1024]{1,0:T(8,128)(2,1)} %wr_ref.1, ...), custom_call_target="tpu_custom_call" | custom-call | tf_op jit(solution)/shard_map/pallas_call | solution.py:794
  149.9 1.7 %copy.44 = bf16[1,64,2048]{2,1,0:T(8,128)(2,1)} copy(bf16[1,64,2048]{2,1,0:T(8,128)(2,1)} %bitcast.18) | data formatting | bytes 524288
  (10 shorter events, 0.1 us)
Async XLA Ops:
  2.0 3.3 %copy-start.2 = (bf16[128,64]{0,1:T(8,128)(2,1)S(1)}, bf16[128,64]{0,1:T(8,128)(2,1)}, u32[]{:S(2)}) copy-start(bf16[128,64]{0,1:T(8,128)(2,1)} %param.26) | copy-start | bytes 49156
  2.0 3.5 %copy-start = (bf16[128,384]{1,0:T(8,128)(2,1)S(1)}, bf16[128,384]{1,0:T(8,128)(2,1)}, u32[]{:S(2)}) copy-start(bf16[128,384]{1,0:T(8,128)(2,1)} %param.24) | copy-start | bytes 294916
  2.0 3.5 %copy-start.1 = (bf16[128,256]{1,0:T(8,128)(2,1)S(1)}, bf16[128,256]{1,0:T(8,128)(2,1)}, u32[]{:S(2)}) copy-start(bf16[128,256]{1,0:T(8,128)(2,1)} %param.25) | copy-start | bytes 196612
  4.0 4.4 %copy-start.3 = (f32[768]{0:T(1024)S(1)}, f32[768]{0:T(1024)}, u32[]{:S(2)}) copy-start(f32[768]{0:T(1024)} %param.29) | copy-start | bytes 9220
  4.0 5.0 %copy-start.4 = (f32[4]{0:T(128)S(1)}, f32[4]{0:T(128)}, u32[]{:S(2)}) copy-start(f32[4]{0:T(128)} %param.35) | copy-start | bytes 52

commit v3 on v2

--- a/solution.py
+++ b/solution.py
@@ -1,4 +1,6 @@
 import functools
+
+import numpy as np
 
 import jax
 import jax.numpy as jnp
@@ -286,17 +288,27 @@
 FIRST, LATER = (0, 1), (2, 3)
 
 
-def heads_fit(mesh, ret_local, sequences, q_wide, kv_wide):
+def heads_fit(mesh, ret_local, sequences, q_wide, kv_wide, up_wide):
     sizes = mesh.shape
     return (
-        sizes["fs"] == 4
+        sizes["sp"] == 4
+        and sizes["fs"] == 4
         and sizes["tp"] == 2
         and ret_local == sizes["sp"]
         and sequences == 1
+        and up_wide == 2 * (NOPE_DIM + ROPE_DIM) * ret_local
         and q_wide % 128 == 0
         and kv_wide % 128 == 0
         and q_wide + kv_wide + 2 * ROPE_DIM <= ret_local * WIDE
     )
+
+
+def wave_tables(length, wide):
+    half_wide = wide // 2
+    powers = np.arange(half_wide, dtype=np.float32) * np.float32(2.0 / wide)
+    inverse = np.power(np.float32(THETA_BASE), -powers).astype(np.float32)
+    angles = np.arange(length, dtype=np.float32)[:, None] * inverse[None, :]
+    return np.cos(angles), np.sin(angles)
 
 
 def three_parts(x):
@@ -348,6 +360,7 @@
     expanded,
     rope_key,
     kvup,
+    qup,
     merged,
     own_sum,
     pair_out,
@@ -365,6 +378,11 @@
     f_recv,
     m_send,
     m_recv,
+    l_send,
+    l_recv,
+    l_relay,
+    p_send,
+    p_recv,
 ):
     z, f, t = lax.axis_index("sp"), lax.axis_index("fs"), lax.axis_index("tp")
     xn = f + 1 - 2 * (f % 2)
@@ -417,13 +435,84 @@
         return (z + n_sp - d) % n_sp
 
     mine = pl.ds(pl.multiple_of(t * half, half), half)
-    tok_copies, z_copies, x_copies, y_copies, f_copies = {}, {}, {}, {}, {}
-    for d in range(1, n_sp):
-        to = (z + d) % n_sp
-        tok_copies[d] = remote(
-            tok_ref.at[mine], tok_all.at[z, mine], m_send.at[0, d], m_recv.at[0, d], sp=to
-        )
-        tok_copies[d].start()
+    z_copies, x_copies, y_copies, f_copies = {}, {}, {}, {}
+
+    def tok_part(origin):
+        return tok_all.at[origin, mine]
+
+    def lat_part(i):
+        return lambda origin: lat_all.at[t, origin, pl.ds(i * rows, rows)]
+
+    def direct(dest):
+        near = (z - dest == 1) | (dest - z == 1)
+        return near if dest in (0, n_sp - 1) else z != dest
+
+    def line_copy(where, row, dest, src=None):
+        return remote(
+            where(z) if src is None else src,
+            where(z),
+            l_send.at[row, dest],
+            l_recv.at[row, z],
+            sp=dest,
+        )
+
+    def relay_copy(where, row, origin, dest):
+        ref = where(origin)
+        return remote(ref, ref, l_relay.at[row, origin], l_recv.at[row, origin], sp=dest)
+
+    def pair_copy(where, row, origin):
+        ref = where(origin)
+        return remote(ref, ref, p_send.at[row, origin], p_recv.at[row, origin], tp=other)
+
+    def line_start(where, row, src=None, pair=True):
+        for dest in range(n_sp):
+            pl.when(direct(dest))(lambda dest=dest: line_copy(where, row, dest, src).start())
+        if pair:
+            for origin in range(n_sp):
+                pl.when(origin == z)(
+                    lambda origin=origin: pair_copy(where, row, origin).start()
+                )
+
+    def passes_on(origin):
+        if origin < n_sp // 2:
+            return z == n_sp - 2, n_sp - 1
+        return z == 1, 0
+
+    def line_pass(where, row):
+        for origin in range(n_sp):
+
+            @pl.when(origin != z)
+            def _(origin=origin):
+                relay_copy(where, row, origin, 0).wait_recv()
+                should, dest = passes_on(origin)
+                pl.when(should)(lambda: relay_copy(where, row, origin, dest).start())
+                pair_copy(where, row, origin).start()
+
+    def pair_arrive(where, row, own):
+        for origin in range(n_sp):
+            if own:
+                pair_copy(where, row, origin).wait_recv()
+            else:
+                pl.when(origin != z)(
+                    lambda origin=origin: pair_copy(where, row, origin).wait_recv()
+                )
+
+    def line_drain(where, row, own):
+        for other_z in range(n_sp):
+            pl.when(direct(other_z))(
+                lambda dest=other_z: line_copy(where, row, dest).wait_send()
+            )
+            if own:
+                pair_copy(where, row, other_z).wait_send()
+
+            @pl.when(other_z != z)
+            def _(origin=other_z):
+                should, dest = passes_on(origin)
+                pl.when(should)(lambda: relay_copy(where, row, origin, dest).wait_send())
+                if not own:
+                    pair_copy(where, row, origin).wait_send()
+
+    line_start(tok_part, 0, tok_ref.at[mine], pair=False)
     for d in range(1, n_sp):
         to = (z + d) % n_sp
         go(remote(shift_ref, shift_all.at[z], m_send.at[2, d], m_recv.at[2, d], sp=to))
@@ -445,6 +534,13 @@
         local_sem.at[8],
     )
     own_kvup.start()
+    up_wide = qup.shape[1]
+    own_qup = pltpu.make_async_copy(
+        qup_ref.at[:, pl.ds(pl.multiple_of(z * up_wide, up_wide), up_wide)],
+        qup,
+        local_sem.at[10],
+    )
+    own_qup.start()
     own_state = pltpu.make_async_copy(start_ref.at[z], state, local_sem.at[9])
     own_state.start()
     for group in (FIRST, LATER):
@@ -490,6 +586,8 @@
             f_copies[d, g].wait_recv()
 
     def at(i):
+        if isinstance(i, int):
+            return slice(i * rows, (i + 1) * rows)
         return pl.ds(pl.multiple_of(i * rows, rows), rows)
 
     def norm_block(i):
@@ -500,15 +598,12 @@
     spread(0, FIRST)
     own_tok.wait()
     norm_block(z)
-    tok_pair = {}
-    for d in range(1, n_sp):
-        tok_copies[d].wait_recv()
-        ref = tok_all.at[owner(d), mine]
-        tok_pair[d] = go(remote(ref, ref, m_send.at[1, d], m_recv.at[1, d], tp=other))
+    line_pass(tok_part, 0)
     for d in range(1, n_sp):
         spread(d, FIRST)
         relay(d - 1, FIRST)
-        tok_pair[d].wait_recv()
+        if d == 1:
+            pair_arrive(tok_part, 0, False)
         norm_block(owner(d))
     relay(n_sp - 1, FIRST)
     spread(0, LATER)
@@ -548,15 +643,9 @@
         lat_all[t, z, at(i), :] = jnp.concatenate(pieces, axis=1).astype(bf16)
         return carry
 
-    lax.fori_loop(0, n_sp, finish_lat, 0)
-    lat_copies = {}
-    lat_own = lat_all.at[t, z]
-    lat_pair = {0: go(remote(lat_own, lat_own, m_send.at[4, 0], m_recv.at[4, 0], tp=other))}
-    for d in range(1, n_sp):
-        lat_copies[d] = remote(
-            lat_own, lat_own, m_send.at[3, d], m_recv.at[3, d], sp=(z + d) % n_sp
-        )
-        lat_copies[d].start()
+    for i in range(n_sp):
+        finish_lat(i, 0)
+        line_start(lat_part(i), i + 1)
 
     def finish_ret(i, carry):
         cosine, sine = rcos_ref[at(i), :], rsin_ref[at(i), :]
@@ -577,9 +666,11 @@
     c_iota = lax.broadcasted_iota(jnp.int32, (rows, rows), 1)
 
     def retention(b):
-        rates = shift_all[b] + rate_ref[...]
+        rates = shift_all[b]
         pick = lax.broadcasted_iota(jnp.int32, rates.shape, 0) == z
-        row = jnp.sum(jnp.where(pick, rates, 0.0), axis=0, keepdims=True)
+        chosen = lax.broadcasted_iota(jnp.int32, rate_ref.shape, 1) == z
+        rate = jnp.sum(jnp.where(chosen, rate_ref[...], 0.0), axis=1, keepdims=True)
+        row = jnp.sum(jnp.where(pick, rates, 0.0), axis=0, keepdims=True) + rate
         column = jnp.sum(jnp.where(r_iota == c_iota, row, 0.0), axis=1, keepdims=True)
         c_col = jnp.sum(jnp.where(c_iota <= r_iota, row, 0.0), axis=1, keepdims=True)
         c_row = jnp.sum(jnp.where(r_iota <= c_iota, column, 0.0), axis=0, keepdims=True)
@@ -610,14 +701,11 @@
         if b:
             spread(b, LATER)
             relay(b - 1, LATER)
-            lat_copies[b].wait_recv()
-            ref = lat_all.at[t, owner(b)]
-            lat_pair[b] = go(remote(ref, ref, m_send.at[4, b], m_recv.at[4, b], tp=other))
+        line_pass(lat_part(b), b + 1)
         retention(b)
     relay(n_sp - 1, LATER)
-    for d in range(n_sp):
-        lat_pair[d].wait_recv()
     own_kvup.wait()
+    own_qup.wait()
 
     def chunks(first, count):
         found = []
@@ -641,21 +729,70 @@
             scaled = x * lax.rsqrt(jnp.mean(x * x, axis=-1, keepdims=True) + EPSILON)
             return (scaled * gain[...]).astype(bf16)
 
-        query = jnp.dot(latent(q_chunks, qgain_ref), qup_ref[...], preferred_element_type=f32)
-        qn[at(i), :] = query[:, :nope].astype(bf16)
-        qr[at(i), :] = (
-            query[:, nope : nope + turn] * pcos_ref[at(i), :]
-            + query[:, nope + turn :] * psin_ref[at(i), :]
-        ).astype(bf16)
+        query = jnp.dot(latent(q_chunks, qgain_ref), qup[...], preferred_element_type=f32)
+        first, middle, end = query[:, :128], query[:, 128:256], query[:, 256:]
+        lane = lax.broadcasted_iota(jnp.int32, first.shape, 1)
+        second = jnp.where(
+            lane < ROPE_DIM, pltpu.roll(middle, ROPE_DIM, 1), pltpu.roll(end, ROPE_DIM, 1)
+        )
+        pair = jnp.where(lane < ROPE_DIM, middle, end)
+        quarter = ROPE_DIM // 2
+        swapped = jnp.where(
+            lane % ROPE_DIM < quarter,
+            pltpu.roll(pair, 2 * ROPE_DIM - quarter, 1),
+            pltpu.roll(pair, quarter, 1),
+        )
+        qn[at(i), :NOPE_DIM] = first.astype(bf16)
+        qn[at(i), NOPE_DIM:] = second.astype(bf16)
+        qr[at(i), :] = (pair * pcos_ref[at(i), :] + swapped * psin_ref[at(i), :]).astype(bf16)
         expanded[at(i), :] = jnp.dot(
             latent(kv_chunks, kvgain_ref), kvup[...], preferred_element_type=f32
         ).astype(bf16)
         rope_key[at(i), :] = lat_all[0, rope_at[0], at(i), rope_at[1] : rope_at[1] + 128]
         return carry
 
-    lax.fori_loop(0, n_sp, expand, 0)
+    for i in range(n_sp):
+        pair_arrive(lat_part(i), i + 1, True)
+        expand(i, 0)
+    for d in range(n_sp):
+        arrive(d, LATER)
+    theirs = pl.ds(pl.multiple_of(other * half, half), half)
+    pair_copies = {}
+
+    def row_copy(b, origin):
+        return remote(row_out.at[b], row_in.at[origin], m_send.at[6, b], m_recv.at[6, origin], sp=b)
+
+    def project_out(b):
+        for which in (theirs, mine):
+            start = pl.multiple_of(b * rows + which.start, half)
+            got = lax.dot_general(
+                merged[pl.ds(start, half), :],
+                w_all[:, 4 * WIDE :],
+                CONTRACT,
+                preferred_element_type=f32,
+            )
+            if which is theirs:
+                pair_out[b] = got.astype(bf16)
+                pair_copies[b] = remote(
+                    pair_out.at[b], pair_in.at[b], m_send.at[5, b], m_recv.at[5, b], tp=other
+                )
+                pair_copies[b].start()
+            else:
+                own_sum[b] = got
+
+    def send_rows(b):
+        pair_copies[b].wait_recv()
+        total = own_sum[b] + pair_in[b].astype(f32)
+        own_sum[b] = total
+
+        @pl.when(z != b)
+        def _():
+            row_out[b] = total.astype(bf16)
+            row_copy(b, z).start()
+
     scale = (NOPE_DIM + ROPE_DIM) ** (-0.5)
-    for b in range(n_sp):
+    order = (0, n_sp - 1) + tuple(range(1, n_sp - 1))
+    for step, b in enumerate(order):
         seen = (b + 1) * rows
         block = slice(b * rows, seen)
         q_at = lax.broadcasted_iota(jnp.int32, (rows, seen), 0) + b * rows
@@ -686,55 +823,24 @@
                 scaled * gain
             ).astype(bf16)
 
-    for d in range(n_sp):
-        arrive(d, LATER)
-    theirs = pl.ds(pl.multiple_of(other * half, half), half)
-    pair_copies, row_copies = {}, {}
-    order = list(range(1, n_sp)) + [0]
-    for d in order:
-        target = (z + d) % n_sp
-        start = pl.multiple_of(target * rows, rows)
-        for which in (theirs, mine):
-            got = lax.dot_general(
-                merged[pl.ds(pl.multiple_of(start + which.start, half), half), :],
-                w_all[:, 4 * WIDE :],
-                CONTRACT,
-                preferred_element_type=f32,
-            )
-            if which is theirs:
-                pair_out[d] = got.astype(bf16)
-                pair_copies[d] = remote(
-                    pair_out.at[d], pair_in.at[d], m_send.at[5, d], m_recv.at[5, d], tp=other
-                )
-                pair_copies[d].start()
-            else:
-                own_sum[d] = got
-    for d in order:
-        pair_copies[d].wait_recv()
-        total = own_sum[d] + pair_in[d].astype(f32)
-        if d:
-            row_out[d] = total.astype(bf16)
-            row_copies[d] = remote(
-                row_out.at[d],
-                row_in.at[d],
-                m_send.at[6, d],
-                m_recv.at[6, d],
-                sp=(z + d) % n_sp,
-            )
-            row_copies[d].start()
-        else:
-            own_sum[0] = total
-    total = own_sum[0]
+        project_out(b)
+        if step:
+            send_rows(order[step - 1])
+    send_rows(order[-1])
+    total = own_sum[z]
     for d in range(1, n_sp):
-        row_copies[d].wait_recv()
-        total = total + row_in[d].astype(f32)
+        row_copy(0, owner(d)).wait_recv()
+        total = total + row_in[owner(d)].astype(f32)
     out_ref[...] = total.astype(bf16)
 
-    sent = pending + [c for group in (
-        tok_copies, z_copies, x_copies, y_copies, f_copies, lat_copies, pair_copies, row_copies
-    ) for c in group.values()]
-    for copy in sent:
-        copy.wait_send()
+    for group in (z_copies, x_copies, y_copies, f_copies, pair_copies):
+        for copy in group.values():
+            copy.wait_send()
+    line_drain(tok_part, 0, False)
+    for i in range(n_sp):
+        line_drain(lat_part(i), i + 1, True)
+    for b in range(n_sp):
+        pl.when(z != b)(lambda b=b: row_copy(b, z).wait_send())
 
 
 def heads_plan(
@@ -759,7 +865,6 @@
     start_state,
 ):
     n_sp = lax.axis_size("sp")
-    z = lax.axis_index("sp")
     rows, width = tokens.shape[1:]
     length = n_sp * rows
     q_wide, kv_wide = w_q_down.shape[1], w_kv_down.shape[1]
@@ -772,18 +877,10 @@
 
     lat = jnp.concatenate([w_q_down, w_kv_down, w_rope_key, swap(w_rope_key)], axis=1)
     lat = jnp.pad(lat, ((0, 0), (0, n_sp * WIDE - lat.shape[1])))
-    head_wide = NOPE_DIM + ROPE_DIM
-    q_up = lax.dynamic_slice_in_dim(w_q_up, z * att_heads * head_wide, att_heads * head_wide, 1)
-    q_up = q_up.reshape(-1, att_heads, head_wide)
-    turned = q_up[..., NOPE_DIM:]
-    q_up = jnp.concatenate(
-        [a.reshape(a.shape[0], -1) for a in (q_up[..., :NOPE_DIM], turned, swap(turned))], axis=1
-    )
-    positions = jnp.arange(length, dtype=jnp.int32)
-    ret_cos, ret_sin = angle_tables(positions, RET_DIM)
-    rope_cos, rope_sin = angle_tables(positions, ROPE_DIM)
-    pair_cos = jnp.concatenate([rope_cos] * 4, axis=1)
-    pair_sin = jnp.concatenate([-rope_sin, rope_sin] * 2, axis=1)
+    ret_cos, ret_sin = wave_tables(length, RET_DIM)
+    rope_cos, rope_sin = wave_tables(length, ROPE_DIM)
+    pair_cos = np.concatenate([rope_cos] * 4, axis=1)
+    pair_sin = np.concatenate([-rope_sin, rope_sin] * 2, axis=1)
     dma = pltpu.SemaphoreType.DMA
     vmem = pltpu.VMEM
     f32, bf16 = jnp.float32, jnp.bfloat16
@@ -794,7 +891,7 @@
     mixed = pl.pallas_call(
         functools.partial(layer_kernel, n_sp, q_wide, kv_wide),
         out_shape=jax.ShapeDtypeStruct((half, out_wide), bf16),
-        in_specs=[any_spec] * 8 + [vmem_spec] * 11 + [any_spec] * 2,
+        in_specs=[any_spec] * 8 + [vmem_spec] * 10 + [any_spec] * 3,
         out_specs=vmem_spec,
         scratch_shapes=[
             vmem((n_sp, rows, width), bf16),
@@ -812,13 +909,14 @@
             vmem((length, att_heads * (NOPE_DIM + VAL_DIM)), bf16),
             vmem((length, 2 * ROPE_DIM), bf16),
             vmem((w_kv_up.shape[0], att_heads * (NOPE_DIM + VAL_DIM)), bf16),
+            vmem((w_q_up.shape[0], att_heads * (NOPE_DIM + ROPE_DIM)), bf16),
             vmem((length, WIDE + att_heads * VAL_DIM), bf16),
             vmem((n_sp, half, out_wide), f32),
             vmem((n_sp, half, out_wide), bf16),
             vmem((n_sp, half, out_wide), bf16),
             vmem((n_sp, half, out_wide), bf16),
             vmem((n_sp, half, out_wide), bf16),
-            dma((10,)),
+            dma((11,)),
             dma((n_sp, 6)),
             dma((n_sp, 6)),
             dma((n_sp, 4)),
@@ -829,6 +927,11 @@
             dma((n_sp, 4)),
             dma((7, n_sp)),
             dma((7, n_sp)),
+            dma((n_sp + 1, n_sp)),
+            dma((n_sp + 1, n_sp)),
+            dma((n_sp + 1, n_sp)),
+            dma((n_sp + 1, n_sp)),
+            dma((n_sp + 1, n_sp)),
         ],
         compiler_params=pltpu.CompilerParams(
             collective_id=0, has_side_effects=True, vmem_limit_bytes=62 * 1024 * 1024
@@ -842,7 +945,7 @@
         w_ret_out,
         w_att_out,
         decay_shift[0],
-        head_rate[:, None],
+        head_rate[None],
         norm_gain[None],
         q_lat_gain[None],
         kv_lat_gain[None],
@@ -852,7 +955,7 @@
         ret_sin,
         pair_cos,
         pair_sin,
-        q_up,
+        w_q_up,
         w_kv_up,
         start_state[0],
     )
@@ -884,7 +987,7 @@
 
     def pick(*args):
         if heads_fit(
-            mesh, args[16].shape[0], args[0].shape[0], args[5].shape[1], args[6].shape[1]
+            mesh, args[16].shape[0], args[0].shape[0], args[5].shape[1], args[6].shape[1], args[8].shape[1]
         ):
             return heads_plan(*args)
         return rows_plan(*args)

time: 152 us -> 134 us (0.88)
  the two profiles are of different devices: /device:TPU:27 before, /device:TPU:0 now
where the time goes in v3:
time: 134 us; the launch traced here: 133 us
  Pallas kernels  127 us (95%)
  local copies, waits for them, and re-layouts  5.58 us (4%)
    pallas_call x1, Pallas kernels, heads_plan(): pl.pallas_call(functools.partial(layer_kernel, n_sp, q_wide, kv_wide), ou...  127 us

profile of v3, /device:TPU:0, one launch (start us, length us, event | category | flops | bytes accessed | tf_op | source)
XLA Modules:
  0.0 133.0 jit_solution(16203952934741571821)
XLA Ops:
  0.0 1.3 broadcast_in_dim.17.qgain_ref
  1.3 0.8 copy.26
  2.1 0.1 fusion
  2.2 1.0 concatenate.3
  3.2 0.7 pad.4.lat_ref
  3.9 127.4 %shard_map.217 = bf16[64,2048]{1,0:T(8,128)(2,1)} custom-call(bf16[128,2048]{1,0:T(8,128)(2,1)} %bitcast.11, bf16[128,1024]{1,0:T(8,128)(2,1)} %pad.4.lat_ref, bf16[128,1024]{1,0:T(8,128)(2,1)} %wq_ref.1, bf16[128,1024]{1,0:T(8,128)(2,1)} %wk_ref.1, bf16[128,1024]{1,0:T(8,128)(2,1)} %wv_ref.1, bf16[128,1024]{1,0:T(8,128)(2,1)} %wr_ref.1, ...), custom_call_target="tpu_custom_call" | custom-call | tf_op jit(solution)/shard_map/pallas_call | solution.py:891
  131.4 1.7 %copy.28 = bf16[1,64,2048]{2,1,0:T(8,128)(2,1)} copy(bf16[1,64,2048]{2,1,0:T(8,128)(2,1)} %bitcast.10) | data formatting | bytes 524288

commit v4 on v3

--- a/solution.py
+++ b/solution.py
@@ -613,18 +613,19 @@
         begin = pl.multiple_of(owner(d) * depth, depth)
 
         def multiply(i, carry, d=d, begin=begin):
+            columns = pl.ds(pl.multiple_of(i * WIDE, WIDE), WIDE)
             got = jnp.dot(
-                normed[at(i), pl.ds(begin, depth)],
-                w_all[pl.ds(begin, depth), : 4 * WIDE],
+                normed[:, pl.ds(begin, depth)],
+                w_all[pl.ds(begin, depth), columns],
                 preferred_element_type=f32,
             )
             if d == 0:
-                acc[at(i), :] = got
+                acc[:, columns] = got
             else:
-                acc[at(i), :] += got
+                acc[:, columns] += got
             return carry
 
-        lax.fori_loop(0, n_sp, multiply, 0)
+        lax.fori_loop(0, 4, multiply, 0)
 
     rope_index = (q_wide + kv_wide) // WIDE
     rope_lane = (q_wide + kv_wide) % WIDE
@@ -756,29 +757,25 @@
         expand(i, 0)
     for d in range(n_sp):
         arrive(d, LATER)
-    theirs = pl.ds(pl.multiple_of(other * half, half), half)
     pair_copies = {}
 
     def row_copy(b, origin):
         return remote(row_out.at[b], row_in.at[origin], m_send.at[6, b], m_recv.at[6, origin], sp=b)
 
     def project_out(b):
-        for which in (theirs, mine):
-            start = pl.multiple_of(b * rows + which.start, half)
-            got = lax.dot_general(
-                merged[pl.ds(start, half), :],
-                w_all[:, 4 * WIDE :],
-                CONTRACT,
-                preferred_element_type=f32,
-            )
-            if which is theirs:
-                pair_out[b] = got.astype(bf16)
-                pair_copies[b] = remote(
-                    pair_out.at[b], pair_in.at[b], m_send.at[5, b], m_recv.at[5, b], tp=other
-                )
-                pair_copies[b].start()
-            else:
-                own_sum[b] = got
+        got = lax.dot_general(
+            merged[b * rows : (b + 1) * rows, :],
+            w_all[:, 4 * WIDE :],
+            CONTRACT,
+            preferred_element_type=f32,
+        )
+        front, back = got[:half, :], got[half:, :]
+        pair_out[b] = jnp.where(t == 0, back, front).astype(bf16)
+        pair_copies[b] = remote(
+            pair_out.at[b], pair_in.at[b], m_send.at[5, b], m_recv.at[5, b], tp=other
+        )
+        pair_copies[b].start()
+        own_sum[b] = jnp.where(t == 0, front, back)
 
     def send_rows(b):
         pair_copies[b].wait_recv()

time: 134 us -> 134 us (level)
  no operation moved by 1% of the time
where the time goes in v4:
time: 134 us; the launch traced here: 132 us
  Pallas kernels  127 us (95%)
  local copies, waits for them, and re-layouts  5.58 us (4%)
    pallas_call x1, Pallas kernels, heads_plan(): pl.pallas_call(functools.partial(layer_kernel, n_sp, q_wide, kv_wide), ou...  127 us

profile of v4, /device:TPU:0, one launch (start us, length us, event | category | flops | bytes accessed | tf_op | source)
XLA Modules:
  0.0 132.4 jit_solution(10227294020020169801)
XLA Ops:
  0.0 1.3 broadcast_in_dim.17.qgain_ref
  1.3 0.8 copy.26
  2.1 0.1 fusion
  2.2 1.0 concatenate.3
  3.2 0.7 pad.4.lat_ref
  3.9 126.8 %shard_map.217 = bf16[64,2048]{1,0:T(8,128)(2,1)} custom-call(bf16[128,2048]{1,0:T(8,128)(2,1)} %bitcast.11, bf16[128,1024]{1,0:T(8,128)(2,1)} %pad.4.lat_ref, bf16[128,1024]{1,0:T(8,128)(2,1)} %wq_ref.1, bf16[128,1024]{1,0:T(8,128)(2,1)} %wk_ref.1, bf16[128,1024]{1,0:T(8,128)(2,1)} %wv_ref.1, bf16[128,1024]{1,0:T(8,128)(2,1)} %wr_ref.1, ...), custom_call_target="tpu_custom_call" | custom-call | tf_op jit(solution)/shard_map/pallas_call | solution.py:888
  130.7 1.7 %copy.28 = bf16[1,64,2048]{2,1,0:T(8,128)(2,1)} copy(bf16[1,64,2048]{2,1,0:T(8,128)(2,1)} %bitcast.10) | data formatting | bytes 524288
